TPU v7x, 32 devices: a whole 2x2x4 slice. The times are simulated.
32 devices in a mesh: kv: 8 (over z, y), tp: 4 (over x, core).
Axes of the slice: x: 2, y: 2, z: 4, core: 2. Of those that a mesh axis runs over, the one named last changes fastest.
Arguments:
- tokens: bfloat16 [16, 4096], P(None, 'tp'), may hold values from -6 to 6
- norm_gain: float32 [4096], P('tp'), may hold values from 0.1 to 1.9
- w_query: bfloat16 [4096, 32, 96], P('tp', 'kv'), as said below
- w_latent: bfloat16 [4096, 1024], P('tp', 'kv'), may hold values from -0.09375 to 0.09375
- w_rotary: bfloat16 [4096, 32], P('tp'), may hold values from -0.09375 to 0.09375
- latent_gain: float32 [1024], replicated, may hold values from 0.1 to 1.9
- w_key_up: bfloat16 [1024, 32, 64], P('tp', 'kv'), may hold values from -0.1875 to 0.1875
- w_value_up: bfloat16 [1024, 32, 128], replicated, may hold values from -0.1875 to 0.1875
- w_out: bfloat16 [4096, 4096], P('kv', 'tp'), may hold values from -0.09375 to 0.09375
- cache_latent: bfloat16 [16, 4096, 1024], P(None, ('kv', 'tp')), may hold values from -6 to 6
- cache_rotary: bfloat16 [16, 4096, 32], P(None, ('kv', 'tp')), may hold values from -6 to 6
- lengths: int32 [16], replicated, may hold values from 1024 to 4096
Outputs:
- mixed_out: bfloat16 [16, 4096], P(None, 'tp')
- new_latent: bfloat16 [16, 1024], P(None, ('kv', 'tp'))
- new_rotary: bfloat16 [16, 32], replicated
Inputs may be any that keep to these rules, and one draw needn't show every extreme that they name: `w_query`: finite.
All inputs are finite; a program needn't handle non-finite values.
Results may differ from a plain program's by a relative error of at most 0.012.
The roundings to bfloat16 on the way count: a program that leaves them out, or rounds other values in their place, can miss the bound.
Values may be sent and summed in bfloat16 or wider, within the bound.
A program may use at most 64 MiB of HBM per device.

v0:
```python
import jax
import jax.numpy as jnp
from jax import lax
from jax.sharding import PartitionSpec as P

THETA = 10000.0
EPS = 1e-06


def rotate(values, position):
    full_width = values.shape[-1]
    half_width = full_width // 2
    frequency = THETA ** (-jnp.arange(0, full_width, 2, dtype=jnp.float32) / full_width)
    angles = position.astype(jnp.float32)[:, None] * frequency[None, :]
    angles = angles.reshape((angles.shape[0],) + (1,) * (values.ndim - 2) + (half_width,))
    cosine = jnp.cos(angles)
    sine_part = jnp.sin(angles)
    first_half = values[..., :half_width]
    second_half = values[..., half_width:]
    return jnp.concatenate(
        [
            first_half * cosine - second_half * sine_part,
            first_half * sine_part + second_half * cosine,
        ],
        axis=-1,
    )


def value_product(latent_f, weight):
    high_part = latent_f.astype(jnp.bfloat16)
    low_part = (latent_f - high_part.astype(jnp.float32)).astype(jnp.bfloat16)
    return jnp.einsum(
        "bhr,rhv->bhv", high_part, weight, preferred_element_type=jnp.float32
    ) + jnp.einsum("bhr,rhv->bhv", low_part, weight, preferred_element_type=jnp.float32)


def shards(
    tokens,
    norm_gain,
    w_query,
    w_latent,
    w_rotary,
    latent_gain,
    w_key_up,
    w_value_up,
    w_out,
    cache_latent,
    cache_rotary,
    lengths,
):
    seq_count = tokens.shape[0]
    kv_count = lax.axis_size("kv")
    tp_count = lax.axis_size("tp")
    kv_index = lax.axis_index("kv")
    tp_index = lax.axis_index("tp")
    heads_dev = w_query.shape[1]
    head_count = heads_dev * kv_count
    latent_rank = cache_latent.shape[2]
    rope_width = cache_rotary.shape[2]
    nope_width = w_query.shape[2] - rope_width
    model_width = tokens.shape[1] * tp_count
    score_scale = w_query.shape[2] ** (-0.5)
    tokens_f = tokens.astype(jnp.float32)
    scaled = (tokens_f * norm_gain).astype(jnp.bfloat16)
    query_part = jnp.einsum("bd,dhn->bhn", scaled, w_query, preferred_element_type=jnp.float32)
    latent_part = jnp.dot(scaled, w_latent, preferred_element_type=jnp.float32)
    rotary_part = jnp.dot(scaled, w_rotary, preferred_element_type=jnp.float32)
    square_part = jnp.sum(tokens_f * tokens_f, axis=1)
    query_sum, latent_sum, rotary_sum, square_sum = lax.psum(
        (query_part, latent_part, rotary_part, square_part), "tp"
    )
    inverse = lax.rsqrt(square_sum / model_width + EPS)
    query_heads = (query_sum * inverse[:, None, None]).astype(jnp.bfloat16)
    compressed = (latent_sum * inverse[:, None]).astype(jnp.bfloat16)
    new_rotary = rotate(rotary_sum * inverse[:, None], lengths).astype(jnp.bfloat16)
    query_rope = rotate(query_heads[:, :, nope_width:].astype(jnp.float32), lengths).astype(
        jnp.bfloat16
    )
    query_latent = jnp.einsum(
        "bhn,rhn->bhr", query_heads[:, :, :nope_width], w_key_up, preferred_element_type=jnp.float32
    ).astype(jnp.bfloat16)
    rope_slice = rope_width // tp_count
    column_slice = compressed.shape[1] // tp_count
    rope_piece = lax.dynamic_slice_in_dim(query_rope, tp_index * rope_slice, rope_slice, 2)
    column_piece = lax.dynamic_slice_in_dim(compressed, tp_index * column_slice, column_slice, 1)
    got_latent, got_rope, got_columns = (
        lax.all_gather(query_latent[:, None], ("kv", "tp"), axis=1, tiled=True),
        lax.all_gather(rope_piece[:, None], ("kv", "tp"), axis=1, tiled=True),
        lax.all_gather(column_piece[:, None], ("kv", "tp"), axis=1, tiled=True),
    )
    rank_slice = query_latent.shape[2]
    all_latent = got_latent.reshape(seq_count, kv_count, tp_count, heads_dev, rank_slice)
    all_latent = all_latent.transpose(0, 1, 3, 2, 4).reshape(seq_count, head_count, latent_rank)
    all_rope = got_rope.reshape(seq_count, kv_count, tp_count, heads_dev, rope_slice)
    all_rope = all_rope.transpose(0, 1, 3, 2, 4).reshape(seq_count, head_count, rope_width)
    fresh_f = got_columns.reshape(seq_count, latent_rank).astype(jnp.float32)
    new_latent = (
        fresh_f * lax.rsqrt(jnp.mean(fresh_f * fresh_f, axis=1, keepdims=True) + EPS) * latent_gain
    ).astype(jnp.bfloat16)
    new_latent_f = new_latent.astype(jnp.float32)
    own_score = (
        jnp.einsum("bhr,br->bh", all_latent, new_latent, preferred_element_type=jnp.float32)
        + jnp.einsum("bhq,bq->bh", all_rope, new_rotary, preferred_element_type=jnp.float32)
    ) * score_scale
    pos_dev = cache_latent.shape[1]
    first_pos = (kv_index * tp_count + tp_index) * pos_dev
    position = first_pos + jnp.arange(pos_dev, dtype=jnp.int32)
    valid = position[None, :] < lengths[:, None]
    scores = (
        jnp.einsum("bhr,bpr->bhp", all_latent, cache_latent, preferred_element_type=jnp.float32)
        + jnp.einsum("bhq,bpq->bhp", all_rope, cache_rotary, preferred_element_type=jnp.float32)
    ) * score_scale
    masked = jnp.where(valid[:, None, :], scores, -jnp.inf)
    local_top = jnp.maximum(jnp.max(masked, axis=2), own_score)
    top_score = lax.pmax(local_top, ("kv", "tp"))
    weights = jnp.where(valid[:, None, :], jnp.exp(scores - top_score[:, :, None]), 0.0)
    total_part = jnp.sum(weights, axis=2)
    summed_part = jnp.einsum(
        "bhp,bpr->bhr",
        weights.astype(jnp.bfloat16),
        cache_latent,
        preferred_element_type=jnp.float32,
    )
    own_weight = jnp.exp(own_score - top_score)
    block_own = lax.dynamic_slice_in_dim(own_weight, kv_index * heads_dev, heads_dev, 1)
    value_block_weight = lax.dynamic_slice_in_dim(w_value_up, kv_index * heads_dev, heads_dev, 1)
    totals, summed = lax.psum((total_part, summed_part), ("kv", "tp"))
    block_sum = lax.dynamic_slice_in_dim(summed, kv_index * heads_dev, heads_dev, 1)
    block_total = lax.dynamic_slice_in_dim(totals, kv_index * heads_dev, heads_dev, 1)
    latent_out = (block_sum + block_own[:, :, None] * new_latent_f[:, None, :]) / (
        block_total + block_own
    )[:, :, None]
    head_out = value_product(latent_out, value_block_weight).astype(jnp.bfloat16)
    out_part = jnp.dot(head_out.reshape(seq_count, -1), w_out, preferred_element_type=jnp.float32)
    mixed_out = lax.psum(out_part, "kv").astype(jnp.bfloat16)
    latent_width = latent_rank // (kv_count * tp_count)
    latent_piece = lax.dynamic_slice_in_dim(
        new_latent, (kv_index * tp_count + tp_index) * latent_width, latent_width, 1
    )
    return (mixed_out, latent_piece, new_rotary)


def solution(mesh):
    placed = (
        P(None, "tp"),
        P("tp"),
        P("tp", "kv", None),
        P("tp", "kv"),
        P("tp", None),
        P(),
        P("tp", "kv", None),
        P(),
        P("kv", "tp"),
        P(None, ("kv", "tp"), None),
        P(None, ("kv", "tp"), None),
        P(),
    )
    return jax.shard_map(
        shards,
        mesh=mesh,
        in_specs=placed,
        out_specs=(P(None, "tp"), P(None, ("kv", "tp")), P()),
        check_vma=False,
    )
```

profile of v0, /device:TPU:0, one launch (start us, length us, event | category | flops | bytes accessed | tf_op | source)
XLA Modules:
  0.0 341.0 jit_solution(9099277364081239508)
XLA Ops:
  7.2 0.0 copy-start
  7.2 0.0 copy-start.2
  7.2 0.0 all-gather.6.cloned.1.call-start
  7.2 1.0 fusion.15
  8.2 1.5 fusion.20
  9.7 1.0 fusion.22
  10.7 1.1 fusion.24
  11.9 13.4 %all-reduce = (f32[16,4,96]{2,0,1:T(8,128)S(1)}, f32[16]{0:T(128)S(1)}, f32[16,128]{1,0:T(8,128)S(1)}, f32[16,32]{1,0:T(8,128)S(1)}) all-reduce(f32[16,4,96]{2,0,1:T(8,128)S(1)} %fusion.20, f32[16]{0:T(128)S(1)} %fusion.15, f32[16,128]{1,0:T(8,128)S(1)} %fusion.24, f32[16,32]{1,0:T(8,128)S(1)} %fusion.22), channel_id=1, replica_groups=mesh['kv'=8,'tp'=4] {'tp'}, use_global_device_ids=true, to_apply=%region_0.0 | all-reduce | flops 8720 | bytes 69760 | tf_op jit(solution)/shard_map/psum | solution.py:69
  25.3 0.1 multiply_convert_fusion.1
  25.3 1.7 fusion.1
  27.0 0.0 all-gather.6.cloned.1.call-update
  27.0 0.0 all-reduce.3.cloned.1.call-start
  27.1 0.7 convert_element_type.81
  27.8 0.1 broadcast_multiply_fusion
  27.8 0.1 subtract_convert_fusion.3
  28.0 0.1 slice_convert_fusion
  28.0 0.1 subtract_convert_fusion.2
  28.1 0.1 dynamic-slice_maximum_fusion
  28.2 0.1 copy.48
  28.3 41.5 %all-gather.1 = bf16[16,128,8]{0,2,1:T(8,128)(2,1)S(1)} all-gather(bf16[16,4,8]{0,2,1:T(8,128)(2,1)S(1)} %copy.48), channel_id=3, replica_groups=mesh['kv'=8,'tp'=4] {'kv','tp'}, dimensions={1}, use_global_device_ids=true | all-gather | bytes 33792 | tf_op jit(solution)/shard_map/all_gather | solution.py:88
  69.8 0.3 copy.50
  70.1 37.0 %all-gather.3 = bf16[32,32,16]{1,2,0:T(8,128)(2,1)S(1)} all-gather(bf16[1,32,16]{1,2,0:T(8,128)(2,1)S(1)} %get-tuple-element.20), channel_id=4, replica_groups=mesh['kv'=8,'tp'=4] {'kv','tp'}, dimensions={0}, use_global_device_ids=true | all-gather | bytes 33792 | tf_op jit(solution)/shard_map/all_gather | solution.py:89
  107.1 0.1 reshape.167
  107.3 0.1 fusion.54
  107.3 0.1 multiply_reduce_fusion
  107.5 0.7 broadcast_compare_fusion
  108.2 0.2 fusion.33
  108.4 0.0 copy-done.2
  108.4 0.1 bitcast_convert_fusion
  108.5 0.0 all-gather.6.cloned.1.call-done
  108.5 2.0 copy.75
  110.5 0.0 copy-start.1
  110.6 0.8 reshape.151
  111.3 3.7 %fusion.41 = f32[16,32,128]{2,1,0:T(8,128)S(1)} fusion(bf16[16,32,1024]{2,1,0:T(8,128)(2,1)S(1)} %reshape.151, bf16[16,128,1024]{2,1,0:T(8,128)(2,1)} %param.21), kind=kOutput, calls=%fused_computation.71 | convolution fusion | flops 134217728 | bytes 5505024 | tf_op jit(solution)/shard_map/bhr,bpr->bhp/dot_general | solution.py:110
  115.0 0.4 fusion.16
  115.4 0.0 copy-done.1
  115.4 0.3 select_reduce_fusion
  115.7 37.0 %pmax.7 = f32[16,32]{1,0:T(8,128)S(1)} all-reduce(f32[16,32]{1,0:T(8,128)S(1)} %get-tuple-element.11), channel_id=1, replica_groups=mesh['kv'=8,'tp'=4] {'kv','tp'}, use_global_device_ids=true, to_apply=%region_7.8 | all-reduce | flops 512 | bytes 4096 | tf_op jit(solution)/shard_map/pmax | solution.py:115
  152.7 2.9 fusion.9
  155.6 2.5 copy.52
  158.2 0.0 all-reduce.3.cloned.1.call-update
  158.2 0.7 pad_maximum_fusion
  158.9 0.7 dynamic-slice_bitcast_fusion
  159.5 2.1 constant_dynamic-slice_fusion
  161.7 0.3 fusion.7
  161.9 42.7 %psum.54 = f32[16,32]{1,0:T(8,128)S(1)} all-reduce(f32[16,32]{1,0:T(8,128)S(1)} %fusion.7), channel_id=1, replica_groups=mesh['kv'=8,'tp'=4] {'kv','tp'}, use_global_device_ids=true, to_apply=%region_10.11 | all-reduce | flops 512 | bytes 4096 | tf_op jit(solution)/shard_map/psum | solution.py:127
  204.6 0.1 dynamic-slice_add_fusion
  204.7 0.1 copy.53
  204.8 0.1 copy.54
  204.8 89.8 %all-reduce.3.cloned.1.call-done = f32[16,32,1024]{2,0,1:T(8,128)} async-done(((f32[16,32,1024]{2,0,1:T(8,128)}), f32[16,32,1024]{2,0,1:T(8,128)}) %all-reduce.3.cloned.1.call-update) | async-done | bytes 2097168 | tf_op jit(solution)/shard_map/psum | solution.py:127
  294.6 1.3 fusion.4
  295.9 1.3 fusion.3
  297.2 0.0 copy-done
  297.2 0.3 fusion.27
  297.4 36.8 %psum.55 = bf16[16,1024]{1,0:T(8,128)(2,1)} all-reduce(f32[16,1024]{1,0:T(8,128)S(1)} %fusion.27), channel_id=1, replica_groups=mesh['kv'=8,'tp'=4] {'kv'}, use_global_device_ids=true, to_apply=%region_11.12 | all-reduce | flops 16384 | bytes 98304 | tf_op jit(solution)/shard_map/psum | solution.py:135
  (7 shorter events, 0.1 us)
Async XLA Ops:
  7.2 290.0 %copy-start = (bf16[512,1024]{1,0:T(8,128)(2,1)S(1)}, bf16[512,1024]{1,0:T(8,128)(2,1)}, u32[]{:S(2)}) copy-start(bf16[512,1024]{1,0:T(8,128)(2,1)} %param.20) | copy-start | bytes 3145732
  7.2 101.2 %copy-start.2 = (f32[1024]{0:T(1024)S(1)}, f32[1024]{0:T(1024)}, u32[]{:S(2)}) copy-start(f32[1024]{0:T(1024)} %param.17) | copy-start | bytes 12292
  7.2 101.3 %all-gather.6.cloned.1.call-start = ((), (), s32[]{:S(2)}) async-start(), calls=%async_computation.1 | async-start | bytes 1081344 | tf_op jit(solution)/shard_map/all_gather | solution.py:87
  27.0 267.6 %all-reduce.3.cloned.1.call-start = ((), (), s32[]{:S(2)}) async-start(), calls=%async_computation | async-start | bytes 4194304 | tf_op jit(solution)/shard_map/psum | solution.py:127
  110.5 4.9 %copy-start.1 = (bf16[16,128,32]{1,2,0:T(8,128)(2,1)S(1)}, bf16[16,128,32]{1,2,0:T(8,128)(2,1)}, u32[]{:S(2)}) copy-start(bf16[16,128,32]{1,2,0:T(8,128)(2,1)} %param.22) | copy-start | bytes 393220
Sparse Core Ops, SparseCore 0:
  27.1 54.0 all-gather.5
  158.3 136.2 all-reduce.2
where the time goes:
time: 342 us; the launch traced here: 341 us
  blocking collectives  208 us (61%)
  waiting for transfers between devices  89.9 us (26%)
  matrix products  15.6 us (5%)
  between operations  14.2 us (4%)
  local copies, waits for them, and re-layouts  8.86 us (3%)
  other arithmetic  4.22 us (1%)
    psum x1, waiting for transfers between devices, shards(): totals, summed = lax.psum((total_part, summed_part), ('kv', 'tp'))  89.8 us
    psum x1, blocking collectives, shards(): totals, summed = lax.psum((total_part, summed_part), ('kv', 'tp'))  42.7 us
    all_gather x1, blocking collectives, shards(): lax.all_gather(rope_piece[:, None], ('kv', 'tp'), axis=1, tiled=True)  41.5 us
    pmax x1, blocking collectives, shards(): top_score = lax.pmax(local_top, ('kv', 'tp'))  37 us
    all_gather x1, blocking collectives, shards(): lax.all_gather(column_piece[:, None], ('kv', 'tp'), axis=1, tiled=True)  37 us
    psum x1, blocking collectives, shards(): mixed_out = lax.psum(out_part, 'kv').astype(jnp.bfloat16)  36.8 us
    psum x1, blocking collectives, shards(): lax.psum((query_part, latent_part, rotary_part, square_part), 'tp')  13.4 us
  transfers between devices with their start and end apart: 2, of which 1 were waited for; matrix products, arithmetic and copies ran while one was open for 2% of the time, Pallas kernels for 0%

commit v1 on v0

--- a/solution.py
+++ b/solution.py
@@ -1,7 +1,14 @@
+import functools
+
 import jax
 import jax.numpy as jnp
 from jax import lax
+from jax.experimental import pallas as pl
+from jax.experimental.pallas import tpu as pltpu
 from jax.sharding import PartitionSpec as P
+
+MESH = pl.DeviceIdType.MESH
+LANES = 128
 
 THETA = 10000.0
 EPS = 1e-06
@@ -32,6 +39,537 @@
     return jnp.einsum(
         "bhr,rhv->bhv", high_part, weight, preferred_element_type=jnp.float32
     ) + jnp.einsum("bhr,rhv->bhv", low_part, weight, preferred_element_type=jnp.float32)
+
+
+def greet(peers):
+    barrier = pltpu.get_barrier_semaphore()
+    for peer in peers:
+        pl.semaphore_signal(barrier, inc=1, device_id=peer, device_id_type=MESH)
+    pl.semaphore_wait(barrier, len(peers))
+
+
+def remote(source, target, send, recv, peer):
+    return pltpu.make_async_remote_copy(
+        src_ref=source,
+        dst_ref=target,
+        send_sem=send,
+        recv_sem=recv,
+        device_id=peer,
+        device_id_type=MESH,
+    )
+
+
+def tp_sum_kernel(tp_count, part_ref, sum_ref, slots, send, recv):
+    kv_index, tp_index = lax.axis_index("kv"), lax.axis_index("tp")
+    peers = [(kv_index, lax.rem(tp_index + step, tp_count)) for step in range(1, tp_count)]
+    greet(peers)
+    copies = []
+    for step, peer in enumerate(peers):
+        copies.append(
+            remote(part_ref, slots.at[tp_index], send.at[step], recv.at[step], peer)
+        )
+        copies[-1].start()
+    slots[tp_index] = part_ref[...]
+    for copy in copies:
+        copy.wait()
+    sum_ref[...] = jnp.sum(slots[...], axis=0)
+
+
+def tp_sum(part, tp_count):
+    return pl.pallas_call(
+        functools.partial(tp_sum_kernel, tp_count),
+        out_shape=jax.ShapeDtypeStruct(part.shape, part.dtype),
+        in_specs=[pl.BlockSpec(memory_space=pltpu.VMEM)],
+        out_specs=pl.BlockSpec(memory_space=pltpu.VMEM),
+        scratch_shapes=[
+            pltpu.VMEM((tp_count,) + part.shape, part.dtype),
+            pltpu.SemaphoreType.DMA((tp_count - 1,)),
+            pltpu.SemaphoreType.DMA((tp_count - 1,)),
+        ],
+        compiler_params=pltpu.CompilerParams(collective_id=0, has_side_effects=True),
+        name="tp_sum",
+    )(part)
+
+
+def chip_offsets(kv_count, tp_count):
+    return [
+        (kv_step, tp_step)
+        for kv_step in range(kv_count)
+        for tp_step in range(0, tp_count, 2)
+        if kv_step + tp_step > 0
+    ]
+
+
+def sibling_of(tp_index):
+    return tp_index + 1 - 2 * lax.rem(tp_index, 2)
+
+
+def gather_kernel(
+    kv_count,
+    tp_count,
+    query_ref,
+    extra_ref,
+    query_out,
+    extra_out,
+    query_all,
+    extra_all,
+    chip_send,
+    chip_recv,
+    pair_send,
+    pair_recv,
+    extra_send,
+    extra_recv,
+):
+    kv_index, tp_index = lax.axis_index("kv"), lax.axis_index("tp")
+    heads, _, width = query_ref.shape
+    offsets = chip_offsets(kv_count, tp_count)
+    sibling = (kv_index, sibling_of(tp_index))
+    greet(
+        [
+            (lax.rem(kv_index + kv_step, kv_count), lax.rem(tp_index + tp_step, tp_count))
+            for kv_step, tp_step in offsets
+        ]
+        + [sibling]
+    )
+
+    def place(kv_at, tp_at):
+        return query_all.at[
+            pl.ds(pl.multiple_of(kv_at * heads, heads), heads),
+            :,
+            pl.ds(pl.multiple_of(tp_at * width, LANES), width),
+        ]
+
+    mine = place(kv_index, tp_index)
+    chip_copies, pair_copies, extra_copies = [], [], []
+    for slot, (kv_step, tp_step) in enumerate(offsets):
+        peer = (lax.rem(kv_index + kv_step, kv_count), lax.rem(tp_index + tp_step, tp_count))
+        chip_copies.append(remote(query_ref, mine, chip_send.at[slot], chip_recv.at[slot], peer))
+        chip_copies[-1].start()
+        if tp_step == 0:
+            extra_copies.append(
+                remote(
+                    extra_ref,
+                    extra_all.at[kv_index],
+                    extra_send.at[kv_step - 1],
+                    extra_recv.at[kv_step - 1],
+                    peer,
+                )
+            )
+            extra_copies[-1].start()
+    last = len(offsets)
+    pair_copies.append(remote(query_ref, mine, pair_send.at[last], pair_recv.at[last], sibling))
+    pair_copies[-1].start()
+    query_all[
+        pl.ds(pl.multiple_of(kv_index * heads, heads), heads),
+        :,
+        pl.ds(pl.multiple_of(tp_index * width, LANES), width),
+    ] = query_ref[...]
+    extra_all[kv_index] = extra_ref[...]
+    for slot, (kv_step, tp_step) in enumerate(offsets):
+        chip_copies[slot].wait_recv()
+        block = place(
+            lax.rem(kv_index - kv_step + kv_count, kv_count),
+            lax.rem(tp_index - tp_step + tp_count, tp_count),
+        )
+        pair_copies.append(remote(block, block, pair_send.at[slot], pair_recv.at[slot], sibling))
+        pair_copies[-1].start()
+    for copy in extra_copies:
+        copy.wait()
+    for copy in chip_copies:
+        copy.wait_send()
+    for copy in pair_copies:
+        copy.wait()
+    query_out[...] = query_all[...]
+    extra_out[...] = extra_all[...]
+
+
+def gather_all(query, extra, kv_count, tp_count):
+    heads, seqs, width = query.shape
+    query_shape = (heads * kv_count, seqs, width * tp_count)
+    extra_shape = (kv_count,) + extra.shape
+    chips = kv_count * tp_count // 2
+    return pl.pallas_call(
+        functools.partial(gather_kernel, kv_count, tp_count),
+        out_shape=(
+            jax.ShapeDtypeStruct(query_shape, query.dtype),
+            jax.ShapeDtypeStruct(extra_shape, extra.dtype),
+        ),
+        in_specs=[pl.BlockSpec(memory_space=pltpu.VMEM)] * 2,
+        out_specs=(pl.BlockSpec(memory_space=pltpu.VMEM),) * 2,
+        scratch_shapes=[
+            pltpu.VMEM(query_shape, query.dtype),
+            pltpu.VMEM(extra_shape, extra.dtype),
+            pltpu.SemaphoreType.DMA((chips - 1,)),
+            pltpu.SemaphoreType.DMA((chips - 1,)),
+            pltpu.SemaphoreType.DMA((chips,)),
+            pltpu.SemaphoreType.DMA((chips,)),
+            pltpu.SemaphoreType.DMA((kv_count - 1,)),
+            pltpu.SemaphoreType.DMA((kv_count - 1,)),
+        ],
+        compiler_params=pltpu.CompilerParams(collective_id=1, has_side_effects=True),
+        name="gather_all",
+    )(query, extra)
+
+
+def split_stats(block, rank):
+    values = block[:, :rank].astype(jnp.float32)
+    stats = block[:, rank:].astype(jnp.float32)
+    top = (stats[:, 0:1] + stats[:, 1:2]) + stats[:, 2:3]
+    return values, top, stats[:, 3:4] + stats[:, 4:5]
+
+
+def merge(first, second):
+    values_a, top_a, total_a = first
+    values_b, top_b, total_b = second
+    top = jnp.maximum(top_a, top_b)
+    scale_a, scale_b = jnp.exp(top_a - top), jnp.exp(top_b - top)
+    return values_a * scale_a + values_b * scale_b, top, total_a * scale_a + total_b * scale_b
+
+
+def rounded(value):
+    return lax.reduce_precision(value, 8, 7)
+
+
+def narrow(value):
+    return value.astype(jnp.bfloat16).astype(jnp.float32)
+
+
+def stats_lanes(top, total, lane, cut):
+    high = cut(top)
+    middle = cut(top - high)
+    low = top - high - middle
+    total_high = cut(total)
+    total_low = total - total_high
+    result = jnp.where(lane == 4, total_low, 0.0)
+    for place, value in enumerate((high, middle, low, total_high)):
+        result = jnp.where(lane == place, value, result)
+    return result
+
+
+def scatter_kernel(
+    kv_count,
+    tp_count,
+    part_ref,
+    sum_ref,
+    stats_ref,
+    from_pair,
+    merged,
+    from_chips,
+    pair_send,
+    pair_recv,
+    chip_send,
+    chip_recv,
+):
+    kv_index, tp_index = lax.axis_index("kv"), lax.axis_index("tp")
+    rank = sum_ref.shape[1]
+    seqs = sum_ref.shape[0]
+    lane = lax.broadcasted_iota(jnp.int32, (seqs, LANES), 1)
+    offsets = chip_offsets(kv_count, tp_count)
+    sibling = (kv_index, sibling_of(tp_index))
+    targets = [
+        (lax.rem(kv_index + kv_step, kv_count), lax.rem(tp_index + tp_step, tp_count))
+        for kv_step, tp_step in offsets
+    ]
+    greet(targets + [sibling])
+    places = targets + [(kv_index, tp_index)]
+    pair_copies, chip_copies = [], []
+    for slot, (kv_at, tp_at) in enumerate(places):
+        pair_copies.append(
+            remote(
+                part_ref.at[kv_at * tp_count + sibling_of(tp_at)],
+                from_pair.at[slot],
+                pair_send.at[slot],
+                pair_recv.at[slot],
+                sibling,
+            )
+        )
+        pair_copies[-1].start()
+    own = None
+    for slot, (kv_at, tp_at) in enumerate(places):
+        pair_copies[slot].wait_recv()
+        values, top, total = merge(
+            split_stats(part_ref[kv_at * tp_count + tp_at], rank),
+            split_stats(from_pair[slot], rank),
+        )
+        if slot == len(targets):
+            own = (values, top, total)
+            continue
+        merged[slot, :, :rank] = values.astype(merged.dtype)
+        merged[slot, :, rank:] = stats_lanes(top, total, lane, narrow).astype(merged.dtype)
+        chip_copies.append(
+            remote(
+                merged.at[slot],
+                from_chips.at[slot],
+                chip_send.at[slot],
+                chip_recv.at[slot],
+                targets[slot],
+            )
+        )
+        chip_copies[-1].start()
+    for slot, copy in enumerate(chip_copies):
+        copy.wait_recv()
+        own = merge(own, split_stats(from_chips[slot], rank))
+    values, top, total = own
+    sum_ref[...] = values
+    stats_ref[...] = jnp.where(lane == 0, top, total)
+    for copy in chip_copies:
+        copy.wait_send()
+    for copy in pair_copies:
+        copy.wait_send()
+
+
+def scatter_sum(part, rank, kv_count, tp_count):
+    _, seqs, width = part.shape
+    chips = kv_count * tp_count // 2
+    return pl.pallas_call(
+        functools.partial(scatter_kernel, kv_count, tp_count),
+        out_shape=(
+            jax.ShapeDtypeStruct((seqs, rank), jnp.float32),
+            jax.ShapeDtypeStruct((seqs, LANES), jnp.float32),
+        ),
+        in_specs=[pl.BlockSpec(memory_space=pltpu.VMEM)],
+        out_specs=(pl.BlockSpec(memory_space=pltpu.VMEM),) * 2,
+        scratch_shapes=[
+            pltpu.VMEM((chips, seqs, width), part.dtype),
+            pltpu.VMEM((chips - 1, seqs, width), part.dtype),
+            pltpu.VMEM((chips - 1, seqs, width), part.dtype),
+            pltpu.SemaphoreType.DMA((chips,)),
+            pltpu.SemaphoreType.DMA((chips,)),
+            pltpu.SemaphoreType.DMA((chips - 1,)),
+            pltpu.SemaphoreType.DMA((chips - 1,)),
+        ],
+        compiler_params=pltpu.CompilerParams(collective_id=2, has_side_effects=True),
+        name="scatter_sum",
+    )(part)
+
+
+def out_kernel(
+    kv_count,
+    tp_count,
+    head_ref,
+    weight_ref,
+    out_ref,
+    heads,
+    parts,
+    got,
+    done,
+    final,
+    head_send,
+    head_recv,
+    part_send,
+    part_recv,
+    done_send,
+    done_recv,
+):
+    kv_index, tp_index = lax.axis_index("kv"), lax.axis_index("tp")
+    depth = head_ref.shape[1]
+    width = parts.shape[2]
+    tp_peers = [(kv_index, lax.rem(tp_index + step, tp_count)) for step in range(1, tp_count)]
+    kv_peers = [(lax.rem(kv_index + step, kv_count), tp_index) for step in range(1, kv_count)]
+    greet(tp_peers + kv_peers)
+    copies = []
+    for step, peer in enumerate(tp_peers):
+        copies.append(
+            remote(head_ref, heads.at[tp_index], head_send.at[step], head_recv.at[step], peer)
+        )
+        copies[-1].start()
+    heads[tp_index] = head_ref[...]
+    for copy in copies:
+        copy.wait()
+    total = jnp.dot(heads[0], weight_ref[:depth, :], preferred_element_type=jnp.float32)
+    for at in range(1, tp_count):
+        total += jnp.dot(
+            heads[at],
+            weight_ref[at * depth : (at + 1) * depth, :],
+            preferred_element_type=jnp.float32,
+        )
+    for at in range(kv_count):
+        parts[at] = total[:, at * width : (at + 1) * width]
+    copies = []
+    for step, peer in enumerate(kv_peers):
+        copies.append(
+            remote(
+                parts.at[peer[0]],
+                got.at[kv_index],
+                part_send.at[step],
+                part_recv.at[step],
+                peer,
+            )
+        )
+        copies[-1].start()
+    got[kv_index] = parts[kv_index]
+    for copy in copies:
+        copy.wait()
+    mine = jnp.sum(got[...], axis=0).astype(out_ref.dtype)
+    done[...] = mine
+    copies = []
+    for step, peer in enumerate(kv_peers):
+        copies.append(
+            remote(done, final.at[kv_index], done_send.at[step], done_recv.at[step], peer)
+        )
+        copies[-1].start()
+    final[kv_index] = mine
+    for copy in copies:
+        copy.wait()
+    for at in range(kv_count):
+        out_ref[:, at * width : (at + 1) * width] = final[at]
+
+
+def project_out(head_out, weight, kv_count, tp_count):
+    seqs, depth = head_out.shape
+    columns = weight.shape[1]
+    width = columns // kv_count
+    return pl.pallas_call(
+        functools.partial(out_kernel, kv_count, tp_count),
+        out_shape=jax.ShapeDtypeStruct((seqs, columns), jnp.bfloat16),
+        in_specs=[pl.BlockSpec(memory_space=pltpu.VMEM)] * 2,
+        out_specs=pl.BlockSpec(memory_space=pltpu.VMEM),
+        scratch_shapes=[
+            pltpu.VMEM((tp_count, seqs, depth), head_out.dtype),
+            pltpu.VMEM((kv_count, seqs, width), jnp.float32),
+            pltpu.VMEM((kv_count, seqs, width), jnp.float32),
+            pltpu.VMEM((seqs, width), jnp.bfloat16),
+            pltpu.VMEM((kv_count, seqs, width), jnp.bfloat16),
+            pltpu.SemaphoreType.DMA((tp_count - 1,)),
+            pltpu.SemaphoreType.DMA((tp_count - 1,)),
+            pltpu.SemaphoreType.DMA((kv_count - 1,)),
+            pltpu.SemaphoreType.DMA((kv_count - 1,)),
+            pltpu.SemaphoreType.DMA((kv_count - 1,)),
+            pltpu.SemaphoreType.DMA((kv_count - 1,)),
+        ],
+        compiler_params=pltpu.CompilerParams(collective_id=3, has_side_effects=True),
+        name="project_out",
+    )(head_out, weight)
+
+
+def kernel_shards(
+    tokens,
+    norm_gain,
+    w_query,
+    w_latent,
+    w_rotary,
+    latent_gain,
+    w_key_up,
+    w_value_up,
+    w_out,
+    cache_latent,
+    cache_rotary,
+    lengths,
+):
+    seq_count = tokens.shape[0]
+    kv_count = lax.axis_size("kv")
+    tp_count = lax.axis_size("tp")
+    kv_index = lax.axis_index("kv")
+    tp_index = lax.axis_index("tp")
+    device = kv_index * tp_count + tp_index
+    heads_dev = w_query.shape[1]
+    head_count = heads_dev * kv_count
+    latent_rank = cache_latent.shape[2]
+    rope_width = cache_rotary.shape[2]
+    nope_width = w_query.shape[2] - rope_width
+    model_width = tokens.shape[1] * tp_count
+    score_scale = w_query.shape[2] ** (-0.5)
+    tokens_f = tokens.astype(jnp.float32)
+    scaled = (tokens_f * norm_gain).astype(jnp.bfloat16)
+    query_part = jnp.einsum("bd,dhn->bhn", scaled, w_query, preferred_element_type=jnp.float32)
+    latent_part = jnp.dot(scaled, w_latent, preferred_element_type=jnp.float32)
+    rotary_part = jnp.dot(scaled, w_rotary, preferred_element_type=jnp.float32)
+    square_part = jnp.sum(tokens_f * tokens_f, axis=1)
+    query_width = heads_dev * w_query.shape[2]
+    latent_width = latent_part.shape[1]
+    fill = -(query_width + latent_width + rope_width) % LANES or LANES
+    packed = jnp.concatenate(
+        [
+            query_part.reshape(seq_count, query_width),
+            latent_part,
+            rotary_part,
+            jnp.broadcast_to(square_part[:, None], (seq_count, fill)),
+        ],
+        axis=1,
+    )
+    packed = tp_sum(packed, tp_count)
+    query_sum, latent_sum, rotary_sum, square_sum = jnp.split(
+        packed,
+        [query_width, query_width + latent_width, query_width + latent_width + rope_width],
+        axis=1,
+    )
+    inverse = lax.rsqrt(square_sum[:, :1] / model_width + EPS)
+    query_heads = (query_sum * inverse).astype(jnp.bfloat16)
+    query_heads = query_heads.reshape(seq_count, heads_dev, w_query.shape[2])
+    compressed = (latent_sum * inverse).astype(jnp.bfloat16)
+    new_rotary = rotate(rotary_sum * inverse, lengths).astype(jnp.bfloat16)
+    query_rope = rotate(query_heads[:, :, nope_width:].astype(jnp.float32), lengths).astype(
+        jnp.bfloat16
+    )
+    query_latent = jnp.einsum(
+        "bhn,rhn->hbr", query_heads[:, :, :nope_width], w_key_up, preferred_element_type=jnp.float32
+    ).astype(jnp.bfloat16)
+    rope_flat = query_rope.reshape(seq_count, heads_dev * rope_width)
+    got_latent, got_extra = gather_all(
+        query_latent, jnp.concatenate([rope_flat, compressed], axis=1), kv_count, tp_count
+    )
+    all_latent = got_latent.transpose(1, 0, 2)
+    all_rope = got_extra[:, :, : heads_dev * rope_width]
+    all_rope = all_rope.reshape(kv_count, seq_count, heads_dev, rope_width)
+    all_rope = all_rope.transpose(1, 0, 2, 3).reshape(seq_count, head_count, rope_width)
+    fresh_f = got_extra[:, :, heads_dev * rope_width :].transpose(1, 0, 2)
+    fresh_f = fresh_f.reshape(seq_count, latent_rank).astype(jnp.float32)
+    new_latent = (
+        fresh_f * lax.rsqrt(jnp.mean(fresh_f * fresh_f, axis=1, keepdims=True) + EPS) * latent_gain
+    ).astype(jnp.bfloat16)
+    new_latent_f = new_latent.astype(jnp.float32)
+    own_score = (
+        jnp.einsum("bhr,br->bh", all_latent, new_latent, preferred_element_type=jnp.float32)
+        + jnp.einsum("bhq,bq->bh", all_rope, new_rotary, preferred_element_type=jnp.float32)
+    ) * score_scale
+    pos_dev = cache_latent.shape[1]
+    position = device * pos_dev + jnp.arange(pos_dev, dtype=jnp.int32)
+    valid = position[None, :] < lengths[:, None]
+    scores = (
+        jnp.einsum("bhr,bpr->bhp", all_latent, cache_latent, preferred_element_type=jnp.float32)
+        + jnp.einsum("bhq,bpq->bhp", all_rope, cache_rotary, preferred_element_type=jnp.float32)
+    ) * score_scale
+    masked = jnp.where(valid[:, None, :], scores, -jnp.inf)
+    local_top = jnp.maximum(jnp.max(masked, axis=2), own_score)
+    weights = jnp.where(valid[:, None, :], jnp.exp(scores - local_top[:, :, None]), 0.0)
+    total_part = jnp.sum(weights, axis=2)
+    summed_part = jnp.einsum(
+        "bhp,bpr->bhr",
+        weights.astype(jnp.bfloat16),
+        cache_latent,
+        preferred_element_type=jnp.float32,
+    ).astype(jnp.bfloat16)
+    lane = lax.broadcasted_iota(jnp.int32, (seq_count, head_count, LANES), 2)
+    stats = stats_lanes(local_top[:, :, None], total_part[:, :, None], lane, rounded)
+    part = jnp.concatenate([summed_part, stats.astype(jnp.bfloat16)], axis=2).transpose(1, 0, 2)
+    block_sum, block_stats = scatter_sum(part, latent_rank, kv_count, tp_count)
+    own = lax.dynamic_slice_in_dim(own_score, device, 1, 1)
+    block_top, block_total = block_stats[:, 0:1], block_stats[:, 1:2]
+    top_score = jnp.maximum(block_top, own)
+    old_scale, own_weight = jnp.exp(block_top - top_score), jnp.exp(own - top_score)
+    latent_out = (block_sum * old_scale + own_weight * new_latent_f) / (
+        block_total * old_scale + own_weight
+    )
+    value_weight = lax.dynamic_slice_in_dim(w_value_up, device, 1, 1)
+    head_out = value_product(latent_out[:, None, :], value_weight).astype(jnp.bfloat16)
+    mixed_out = project_out(head_out[:, 0, :], w_out, kv_count, tp_count)
+    piece_width = latent_rank // (kv_count * tp_count)
+    latent_piece = lax.dynamic_slice_in_dim(new_latent, device * piece_width, piece_width, 1)
+    return (mixed_out, latent_piece, new_rotary)
+
+
+def fits_kernels(args, kv_count, tp_count):
+    w_query, w_latent, w_rotary, w_key_up, w_value_up, w_out = args
+    heads = w_query.shape[1]
+    return (
+        heads == kv_count * tp_count
+        and tp_count % 2 == 0
+        and w_key_up.shape[0] // tp_count % LANES == 0
+        and w_latent.shape[1] // kv_count % LANES == 0
+        and heads // kv_count * w_rotary.shape[1] % LANES == 0
+        and w_value_up.shape[2] % LANES == 0
+        and w_out.shape[1] // tp_count // kv_count % LANES == 0
+    )
 
 
 def shards(
@@ -155,10 +693,16 @@
         P(None, ("kv", "tp"), None),
         P(),
     )
-    return jax.shard_map(
-        shards,
-        mesh=mesh,
-        in_specs=placed,
-        out_specs=(P(None, "tp"), P(None, ("kv", "tp")), P()),
-        check_vma=False,
-    )
+
+    def step(*args):
+        weights = (args[2], args[3], args[4], args[6], args[7], args[8])
+        fits = fits_kernels(weights, mesh.shape["kv"], mesh.shape["tp"])
+        return jax.shard_map(
+            kernel_shards if fits else shards,
+            mesh=mesh,
+            in_specs=placed,
+            out_specs=(P(None, "tp"), P(None, ("kv", "tp")), P()),
+            check_vma=False,
+        )(*args)
+
+    return step

time: 342 us -> 110 us (0.32)
  blocking collectives: 208 us -> 0 us
  waiting for transfers between devices: 89.9 us -> 0 us
  Pallas kernels: 0 us -> 71.1 us
  between operations: 14.2 us -> 0.84 us
  other arithmetic: 4.22 us -> 13.8 us
    psum x3 -> x0, blocking collectives: 92.8 us -> none  [the longest x1 42.7 us: shards(): totals, summed = lax.psum((total_part, summed_part), ('kv', 'tp'))]
    psum x1 -> x0, waiting for transfers between devices: 89.8 us -> none  [shards(): totals, summed = lax.psum((total_part, summed_part), ('kv', 'tp'))]
    all_gather x2 -> x0, blocking collectives: 78.4 us -> none  [the longest x1 41.5 us: shards(): lax.all_gather(rope_piece[:, None], ('kv', 'tp'), axis=1, tiled=True)]
    pallas_call x0 -> x4, Pallas kernels: none -> 71.1 us  [the longest x1 23.8 us: scatter_sum(): pl.pallas_call(functools.partial(scatter_kernel, kv_count, tp_count), out...]
    pmax x1 -> x0, blocking collectives: 37 us -> none  [shards(): top_score = lax.pmax(local_top, ('kv', 'tp'))]
    convert_element_type x3 -> x7, other arithmetic: 0.24 us -> 4.06 us  [the longest x2 1.56 us: kernel_shards(): new_latent = (fresh_f * lax.rsqrt(jnp.mean(fresh_f * fresh_f, axis=1, kee...]
    dot_general x10 -> x9, matrix products: 13 us -> 14 us  [the longest x1 4.03 us: kernel_shards(): jnp.einsum('bhr,bpr->bhp', all_latent, cache_latent, preferred_element_ty...]
  transfers between devices with their start and end apart: 2 -> 0, of which waited for: 1 -> 0; matrix products, arithmetic and copies ran while one was open for 2% -> 0% of each run, Pallas kernels for 0% -> 0%
where the time goes in v1:
time: 110 us; the launch traced here: 109 us
  Pallas kernels  71.1 us (65%)
  matrix products  16.7 us (15%)
  other arithmetic  13.8 us (13%)
  local copies, waits for them, and re-layouts  6.16 us (6%)
    pallas_call x1, Pallas kernels, scatter_sum(): pl.pallas_call(functools.partial(scatter_kernel, kv_count, tp_count), out...  23.8 us
    pallas_call x1, Pallas kernels, project_out(): pl.pallas_call(functools.partial(out_kernel, kv_count, tp_count), out_sha...  21.5 us
    pallas_call x1, Pallas kernels, gather_all(): pl.pallas_call(functools.partial(gather_kernel, kv_count, tp_count), out_...  19 us
    pallas_call x1, Pallas kernels, tp_sum(): pl.pallas_call(functools.partial(tp_sum_kernel, tp_count), out_shape=jax....  6.83 us
    dot_general x1, matrix products, kernel_shards(): jnp.einsum('bhr,bpr->bhp', all_latent, cache_latent, preferred_element_ty...  4.03 us
    dot_general x1, matrix products, kernel_shards(): jnp.einsum('bhp,bpr->bhr', weights.astype(jnp.bfloat16), cache_latent, pr...  2.86 us
    unnamed x9, local copies, waits for them, and re-layouts  2.52 us

profile of v1, /device:TPU:0, one launch (start us, length us, event | category | flops | bytes accessed | tf_op | source)
XLA Modules:
  0.0 108.7 jit_solution(13312660434045085015)
XLA Ops:
  0.6 0.0 copy-start
  0.6 0.0 copy-start.1
  0.7 1.1 %copy-done = bf16[1024,4,96]{0,2,1:T(8,128)(2,1)S(1)} copy-done((bf16[1024,4,96]{0,2,1:T(8,128)(2,1)S(1)}, bf16[1024,4,96]{0,2,1:T(8,128)(2,1)}, u32[]{:S(2)}) %copy-start) | copy-done | bytes 786456
  1.8 1.1 %fusion.18 = f32[16,4,96]{2,0,1:T(8,128)S(1)} fusion(bf16[1024,4,96]{0,2,1:T(8,128)(2,1)S(1)} %copy-done, bf16[16,1024]{1,0:T(8,128)(2,1)} %param.12, f32[1024]{0:T(1024)} %param.13), kind=kOutput, calls=%fused_computation.35 | convolution fusion | flops 12632064 | bytes 847872 | tf_op jit(solution)/shard_map/bd,dhn->bhn/dot_general | solution.py:474
  2.9 0.1 reshape.150
  3.0 0.9 fusion.13
  3.9 0.1 broadcast_in_dim.73
  4.0 1.0 fusion.20
  5.0 1.1 %fusion.22 = f32[16,128]{1,0:T(8,128)S(1)} fusion(bf16[1024,128]{1,0:T(8,128)(2,1)} %param.15, bf16[16,1024]{1,0:T(8,128)(2,1)} %param.12, f32[1024]{0:T(1024)} %param.13), kind=kOutput, calls=%fused_computation.41 | convolution fusion | flops 4243456 | bytes 307200 | tf_op jit(solution)/shard_map/dot_general | solution.py:475
  6.1 0.7 pad_maximum_fusion.part_ref
  6.8 6.8 %tp_sum.1 = f32[16,640]{1,0:T(8,128)} custom-call(f32[16,640]{1,0:T(8,128)} %pad_maximum_fusion.part_ref), custom_call_target="tpu_custom_call" | custom-call | tf_op jit(solution)/shard_map/tp_sum/pallas_call | solution.py:79
  13.6 0.9 rsqrt_reduce_fusion
  14.5 0.8 slice_multiply_fusion
  15.3 0.7 convert_element_type.82
  16.0 0.1 subtract_convert_fusion.3
  16.1 0.8 multiply_convert_fusion
  16.9 0.1 reshape.151
  17.0 0.1 slice_convert_fusion
  17.1 0.1 subtract_convert_fusion.2
  17.2 0.1 pad_maximum_fusion.1
  17.3 0.1 convert_element_type.83
  17.4 0.8 multiply_convert_fusion.1
  18.1 0.6 pad_maximum_fusion.2.extra_ref
  18.7 1.7 %convolution_convert_fusion.query_ref = bf16[4,16,256]{2,1,0:T(8,128)(2,1)} fusion(bf16[256,4,64]{0,2,1:T(8,128)(2,1)} %param.18, bf16[16,4,64]{2,1,0:T(4,128)(2,1)S(1)} %bitcast.51), kind=kOutput, calls=%fused_computation.2 | convolution fusion | flops 2113536 | bytes 172032 | tf_op jit(solution)/shard_map/bhn,rhn->hbr/dot_general | solution.py:504
  20.4 19.0 %gather_all.1 = (bf16[32,16,1024]{2,1,0:T(8,128)(2,1)}, bf16[8,16,256]{2,1,0:T(8,128)(2,1)}) custom-call(bf16[4,16,256]{2,1,0:T(8,128)(2,1)} %convolution_convert_fusion.query_ref, bf16[16,256]{1,0:T(8,128)(2,1)} %pad_maximum_fusion.2.extra_ref), custom_call_target="tpu_custom_call" | custom-call | tf_op jit(solution)/shard_map/gather_all/pallas_call | solution.py:191
  39.4 0.8 fusion.34
  40.2 0.9 fusion.14
  41.0 0.8 fusion.16
  41.8 0.7 pad_maximum_fusion.3
  42.5 0.0 copy-start.2
  42.5 0.1 reshape.152
  42.6 0.0 copy-start.3
  42.7 0.2 fusion.30
  42.8 0.8 fusion.46
  43.6 1.9 %fusion.2 = f32[16,1,32]{2,1,0:T(1,128)S(1)} fusion(bf16[16,32,1024]{2,0,1:T(8,128)(2,1)} %bitcast.46, bf16[16,1024,1]{1,0,2:T(8,128)(2,1)S(1)} %fusion.46), kind=kOutput, calls=%fused_computation.6 | convolution fusion | flops 1048576 | bytes 1083392 | tf_op jit(solution)/shard_map/bhr,br->bh/dot_general | solution.py:522
  45.5 0.0 copy-done.1
  45.5 0.2 fusion.36
  45.7 4.0 %fusion.4 = f32[16,32,128]{2,1,0:T(8,128)S(1)} fusion(bf16[16,128,1024]{2,1,0:T(8,128)(2,1)} %param.21, bf16[16,32,1024]{2,0,1:T(8,128)(2,1)} %bitcast.47), kind=kOutput, calls=%fused_computation.8 | convolution fusion | flops 134217728 | bytes 5505024 | tf_op jit(solution)/shard_map/bhr,bpr->bhp/dot_general | solution.py:529
  49.7 0.0 copy-done.2
  49.7 0.0 copy-done.3
  49.8 0.1 broadcast_compare_fusion
  49.8 0.4 select_reduce_fusion
  50.2 0.1 copy.50
  50.3 0.1 copy.51
  50.4 0.4 fusion.8
  50.8 2.9 %fusion.9 = bf16[16,32,1024]{2,1,0:T(8,128)(2,1)S(1)} fusion(bf16[16,128,1024]{2,1,0:T(8,128)(2,1)} %param.21, bf16[16,32,128]{2,0,1:T(8,128)(2,1)S(1)} %get-tuple-element.17), kind=kOutput, calls=%fused_computation.18 | convolution fusion | flops 134217728 | bytes 5373952 | tf_op jit(solution)/shard_map/bhp,bpr->bhr/dot_general | solution.py:536
  53.7 0.6 copy.97
  54.3 0.1 copy.55
  54.4 0.1 copy.56
  54.5 0.1 copy.54
  54.6 0.4 select_convert_fusion
  55.0 1.1 %maximum_bitcast_fusion.part_ref = bf16[32,16,1152]{2,1,0:T(8,128)(2,1)} fusion(bf16[16,32,128]{2,0,1:T(8,128)(2,1)S(1)} %select_convert_fusion, bf16[16,32,1024]{2,0,1:T(8,128)(2,1)S(1)} %copy.97), kind=kLoop, calls=%fused_computation.1 | loop fusion | flops 2359296 | bytes 2359296 | tf_op jit(solution)/shard_map/transpose | solution.py:544
  56.1 23.8 %scatter_sum.1 = (f32[16,1024]{1,0:T(8,128)}, f32[16,128]{1,0:T(8,128)}) custom-call(bf16[32,16,1152]{2,1,0:T(8,128)(2,1)} %maximum_bitcast_fusion.part_ref), custom_call_target="tpu_custom_call" | custom-call | tf_op jit(solution)/shard_map/scatter_sum/pallas_call | solution.py:324
  80.0 1.0 fusion.33
  81.0 2.1 %constant_dynamic-slice_fusion.1 = bf16[1024,1,128]{2,1,0:T(2,128)(2,1)S(1)} fusion(bf16[1024,32,128]{2,1,0:T(8,128)(2,1)} %param.19, s32[]{:T(128)S(6)} %select_n.31), kind=kLoop, calls=%fused_computation.71 | loop fusion | bytes 524292 | tf_op jit(solution)/shard_map/dynamic_slice | solution.py:553
  83.1 1.1 fusion.11
  84.2 1.7 %fusion.1.head_ref = bf16[16,128]{1,0:T(8,128)(2,1)} fusion(f32[128,16]{0,1:T(8,128)S(1)} %fusion.11, bf16[1024,1,128]{2,1,0:T(2,128)(2,1)S(1)} %constant_dynamic-slice_fusion.1, bf16[16,1024]{1,0:T(8,128)(2,1)S(1)} %fusion.16, f32[16,1024]{1,0:T(8,128)} %get-tuple-element.9, f32[16]{0:T(128)S(1)} %get-tuple-element.12, f32[16]{0:T(128)S(1)} %get-tuple-element.13, ...), kind=kOutput, calls=%fused_computation.5 | convolution fusion | flops 4345856 | bytes 372928 | tf_op jit(solution)/shard_map/bhr,rhv->bhv/dot_general | solution.py:41
  85.8 21.5 %project_out.1 = bf16[16,1024]{1,0:T(8,128)(2,1)} custom-call(bf16[16,128]{1,0:T(8,128)(2,1)} %fusion.1.head_ref, bf16[512,1024]{1,0:T(8,128)(2,1)} %weight_ref.1), custom_call_target="tpu_custom_call" | custom-call | tf_op jit(solution)/shard_map/project_out/pallas_call | solution.py:422
  107.3 1.4 %copy.101 = bf16[16,1024]{1,0:T(8,128)(2,1)} copy(bf16[16,1024]{1,0:T(8,128)(2,1)} %project_out.1) | data formatting | bytes 65536
  (11 shorter events, 0.1 us)
Async XLA Ops:
  0.6 1.1 %copy-start = (bf16[1024,4,96]{0,2,1:T(8,128)(2,1)S(1)}, bf16[1024,4,96]{0,2,1:T(8,128)(2,1)}, u32[]{:S(2)}) copy-start(bf16[1024,4,96]{0,2,1:T(8,128)(2,1)} %param.14) | copy-start | bytes 2359300
  0.6 44.9 %copy-start.1 = (bf16[16,128,32]{1,2,0:T(8,128)(2,1)S(1)}, bf16[16,128,32]{1,2,0:T(8,128)(2,1)}, u32[]{:S(2)}) copy-start(bf16[16,128,32]{1,2,0:T(8,128)(2,1)} %param.22) | copy-start | bytes 393220
  42.5 7.2 %copy-start.2 = (bf16[16,32]{1,0:T(8,128)(2,1)}, bf16[16,32]{1,0:T(8,128)(2,1)S(1)}, u32[]{:S(2)}) copy-start(bf16[16,32]{1,0:T(8,128)(2,1)S(1)} %get-tuple-element.42) | copy-start | bytes 3076
  42.6 7.2 %copy-start.3 = (s32[16]{0:T(128)S(1)}, s32[16]{0:T(128)}, u32[]{:S(2)}) copy-start(s32[16]{0:T(128)} %param.23) | copy-start | bytes 196

commit v2 on v1

--- a/solution.py
+++ b/solution.py
@@ -9,6 +9,8 @@
 
 MESH = pl.DeviceIdType.MESH
 LANES = 128
+INNER = 2
+LOWEST = -1e38
 
 THETA = 10000.0
 EPS = 1e-06
@@ -91,13 +93,16 @@
     )(part)
 
 
-def chip_offsets(kv_count, tp_count):
-    return [
-        (kv_step, tp_step)
-        for kv_step in range(kv_count)
-        for tp_step in range(0, tp_count, 2)
-        if kv_step + tp_step > 0
-    ]
+def plane_offsets(tp_count):
+    return [(inner, step) for inner in range(INNER) for step in range(0, tp_count, 2)]
+
+
+def plane_peer(kv_index, tp_index, tp_count, offset):
+    outer, inner = kv_index // INNER, lax.rem(kv_index, INNER)
+    return (
+        outer * INNER + lax.rem(inner + offset[0], INNER),
+        lax.rem(tp_index + offset[1], tp_count),
+    )
 
 
 def sibling_of(tp_index):
@@ -113,24 +118,32 @@
     extra_out,
     query_all,
     extra_all,
-    chip_send,
-    chip_recv,
+    line_send,
+    line_recv,
+    plane_send,
+    plane_recv,
     pair_send,
     pair_recv,
     extra_send,
     extra_recv,
+    side_send,
+    side_recv,
 ):
     kv_index, tp_index = lax.axis_index("kv"), lax.axis_index("tp")
     heads, _, width = query_ref.shape
-    offsets = chip_offsets(kv_count, tp_count)
+    lines = kv_count // INNER
+    offsets = plane_offsets(tp_count)
+    back = [(-inner % INNER, -step % tp_count) for inner, step in offsets]
     sibling = (kv_index, sibling_of(tp_index))
-    greet(
-        [
-            (lax.rem(kv_index + kv_step, kv_count), lax.rem(tp_index + tp_step, tp_count))
-            for kv_step, tp_step in offsets
-        ]
-        + [sibling]
-    )
+    line_peers = [
+        (lax.rem(kv_index + INNER * step, kv_count), tp_index) for step in range(1, lines)
+    ]
+    planes = [plane_peer(kv_index, tp_index, tp_count, offset) for offset in offsets]
+    sources = [plane_peer(kv_index, tp_index, tp_count, offset) for offset in back]
+    greet(line_peers + planes[1:] + [sibling])
+
+    def shifted(kv_at, step):
+        return lax.rem(kv_at - INNER * step + kv_count, kv_count)
 
     def place(kv_at, tp_at):
         return query_all.at[
@@ -139,46 +152,76 @@
             pl.ds(pl.multiple_of(tp_at * width, LANES), width),
         ]
 
+    copies, line_copies, extra_copies, plane_copies = [], [], [], {}
     mine = place(kv_index, tp_index)
-    chip_copies, pair_copies, extra_copies = [], [], []
-    for slot, (kv_step, tp_step) in enumerate(offsets):
-        peer = (lax.rem(kv_index + kv_step, kv_count), lax.rem(tp_index + tp_step, tp_count))
-        chip_copies.append(remote(query_ref, mine, chip_send.at[slot], chip_recv.at[slot], peer))
-        chip_copies[-1].start()
-        if tp_step == 0:
-            extra_copies.append(
-                remote(
-                    extra_ref,
-                    extra_all.at[kv_index],
-                    extra_send.at[kv_step - 1],
-                    extra_recv.at[kv_step - 1],
-                    peer,
-                )
+    for step, peer in enumerate(line_peers):
+        line_copies.append(remote(query_ref, mine, line_send.at[step], line_recv.at[step], peer))
+        line_copies[-1].start()
+        extra_copies.append(
+            remote(
+                extra_ref, extra_all.at[kv_index], extra_send.at[step], extra_recv.at[step], peer
             )
-            extra_copies[-1].start()
-    last = len(offsets)
-    pair_copies.append(remote(query_ref, mine, pair_send.at[last], pair_recv.at[last], sibling))
-    pair_copies[-1].start()
+        )
+        extra_copies[-1].start()
     query_all[
         pl.ds(pl.multiple_of(kv_index * heads, heads), heads),
         :,
         pl.ds(pl.multiple_of(tp_index * width, LANES), width),
     ] = query_ref[...]
     extra_all[kv_index] = extra_ref[...]
-    for slot, (kv_step, tp_step) in enumerate(offsets):
-        chip_copies[slot].wait_recv()
-        block = place(
-            lax.rem(kv_index - kv_step + kv_count, kv_count),
-            lax.rem(tp_index - tp_step + tp_count, tp_count),
-        )
-        pair_copies.append(remote(block, block, pair_send.at[slot], pair_recv.at[slot], sibling))
-        pair_copies[-1].start()
-    for copy in extra_copies:
+
+    side = plane_peer(kv_index, tp_index, tp_count, (1, 0))
+    side_copies = []
+    for line in range(lines):
+        kv_at = shifted(kv_index, line)
+        target = place(kv_at, tp_index)
+        extra_target = extra_all.at[kv_at]
+        if line > 0:
+            line_copies[line - 1].wait_recv()
+            extra_copies[line - 1].wait_recv()
+        for slot in range(1, len(offsets)):
+            plane_copies[line, slot] = remote(
+                query_ref if line == 0 else target,
+                target,
+                plane_send.at[line, slot],
+                plane_recv.at[line, slot],
+                planes[slot],
+            )
+            plane_copies[line, slot].start()
+        side_copies.append(
+            remote(
+                extra_ref if line == 0 else extra_target,
+                extra_target,
+                side_send.at[line],
+                side_recv.at[line],
+                side,
+            )
+        )
+        side_copies[-1].start()
+        copies.append(
+            remote(
+                query_ref if line == 0 else target,
+                target,
+                pair_send.at[line, 0],
+                pair_recv.at[line, 0],
+                sibling,
+            )
+        )
+        copies[-1].start()
+    for line in range(lines):
+        for slot in range(1, len(offsets)):
+            plane_copies[line, slot].wait_recv()
+            target = place(shifted(sources[slot][0], line), sources[slot][1])
+            copies.append(
+                remote(
+                    target, target, pair_send.at[line, slot], pair_recv.at[line, slot], sibling
+                )
+            )
+            copies[-1].start()
+    for copy in side_copies + copies:
         copy.wait()
-    for copy in chip_copies:
+    for copy in line_copies + extra_copies + list(plane_copies.values()):
         copy.wait_send()
-    for copy in pair_copies:
-        copy.wait()
     query_out[...] = query_all[...]
     extra_out[...] = extra_all[...]
 
@@ -187,7 +230,7 @@
     heads, seqs, width = query.shape
     query_shape = (heads * kv_count, seqs, width * tp_count)
     extra_shape = (kv_count,) + extra.shape
-    chips = kv_count * tp_count // 2
+    lines, planes = kv_count // INNER, INNER * tp_count // 2
     return pl.pallas_call(
         functools.partial(gather_kernel, kv_count, tp_count),
         out_shape=(
@@ -199,12 +242,16 @@
         scratch_shapes=[
             pltpu.VMEM(query_shape, query.dtype),
             pltpu.VMEM(extra_shape, extra.dtype),
-            pltpu.SemaphoreType.DMA((chips - 1,)),
-            pltpu.SemaphoreType.DMA((chips - 1,)),
-            pltpu.SemaphoreType.DMA((chips,)),
-            pltpu.SemaphoreType.DMA((chips,)),
-            pltpu.SemaphoreType.DMA((kv_count - 1,)),
-            pltpu.SemaphoreType.DMA((kv_count - 1,)),
+            pltpu.SemaphoreType.DMA((lines - 1,)),
+            pltpu.SemaphoreType.DMA((lines - 1,)),
+            pltpu.SemaphoreType.DMA((lines, planes)),
+            pltpu.SemaphoreType.DMA((lines, planes)),
+            pltpu.SemaphoreType.DMA((lines, planes)),
+            pltpu.SemaphoreType.DMA((lines, planes)),
+            pltpu.SemaphoreType.DMA((lines - 1,)),
+            pltpu.SemaphoreType.DMA((lines - 1,)),
+            pltpu.SemaphoreType.DMA((lines,)),
+            pltpu.SemaphoreType.DMA((lines,)),
         ],
         compiler_params=pltpu.CompilerParams(collective_id=1, has_side_effects=True),
         name="gather_all",
@@ -250,110 +297,27 @@
     kv_count,
     tp_count,
     part_ref,
-    sum_ref,
-    stats_ref,
+    own_ref,
+    fresh_ref,
+    value_ref,
+    weight_ref,
+    out_ref,
     from_pair,
     merged,
-    from_chips,
-    pair_send,
-    pair_recv,
-    chip_send,
-    chip_recv,
-):
-    kv_index, tp_index = lax.axis_index("kv"), lax.axis_index("tp")
-    rank = sum_ref.shape[1]
-    seqs = sum_ref.shape[0]
-    lane = lax.broadcasted_iota(jnp.int32, (seqs, LANES), 1)
-    offsets = chip_offsets(kv_count, tp_count)
-    sibling = (kv_index, sibling_of(tp_index))
-    targets = [
-        (lax.rem(kv_index + kv_step, kv_count), lax.rem(tp_index + tp_step, tp_count))
-        for kv_step, tp_step in offsets
-    ]
-    greet(targets + [sibling])
-    places = targets + [(kv_index, tp_index)]
-    pair_copies, chip_copies = [], []
-    for slot, (kv_at, tp_at) in enumerate(places):
-        pair_copies.append(
-            remote(
-                part_ref.at[kv_at * tp_count + sibling_of(tp_at)],
-                from_pair.at[slot],
-                pair_send.at[slot],
-                pair_recv.at[slot],
-                sibling,
-            )
-        )
-        pair_copies[-1].start()
-    own = None
-    for slot, (kv_at, tp_at) in enumerate(places):
-        pair_copies[slot].wait_recv()
-        values, top, total = merge(
-            split_stats(part_ref[kv_at * tp_count + tp_at], rank),
-            split_stats(from_pair[slot], rank),
-        )
-        if slot == len(targets):
-            own = (values, top, total)
-            continue
-        merged[slot, :, :rank] = values.astype(merged.dtype)
-        merged[slot, :, rank:] = stats_lanes(top, total, lane, narrow).astype(merged.dtype)
-        chip_copies.append(
-            remote(
-                merged.at[slot],
-                from_chips.at[slot],
-                chip_send.at[slot],
-                chip_recv.at[slot],
-                targets[slot],
-            )
-        )
-        chip_copies[-1].start()
-    for slot, copy in enumerate(chip_copies):
-        copy.wait_recv()
-        own = merge(own, split_stats(from_chips[slot], rank))
-    values, top, total = own
-    sum_ref[...] = values
-    stats_ref[...] = jnp.where(lane == 0, top, total)
-    for copy in chip_copies:
-        copy.wait_send()
-    for copy in pair_copies:
-        copy.wait_send()
-
-
-def scatter_sum(part, rank, kv_count, tp_count):
-    _, seqs, width = part.shape
-    chips = kv_count * tp_count // 2
-    return pl.pallas_call(
-        functools.partial(scatter_kernel, kv_count, tp_count),
-        out_shape=(
-            jax.ShapeDtypeStruct((seqs, rank), jnp.float32),
-            jax.ShapeDtypeStruct((seqs, LANES), jnp.float32),
-        ),
-        in_specs=[pl.BlockSpec(memory_space=pltpu.VMEM)],
-        out_specs=(pl.BlockSpec(memory_space=pltpu.VMEM),) * 2,
-        scratch_shapes=[
-            pltpu.VMEM((chips, seqs, width), part.dtype),
-            pltpu.VMEM((chips - 1, seqs, width), part.dtype),
-            pltpu.VMEM((chips - 1, seqs, width), part.dtype),
-            pltpu.SemaphoreType.DMA((chips,)),
-            pltpu.SemaphoreType.DMA((chips,)),
-            pltpu.SemaphoreType.DMA((chips - 1,)),
-            pltpu.SemaphoreType.DMA((chips - 1,)),
-        ],
-        compiler_params=pltpu.CompilerParams(collective_id=2, has_side_effects=True),
-        name="scatter_sum",
-    )(part)
-
-
-def out_kernel(
-    kv_count,
-    tp_count,
-    head_ref,
-    weight_ref,
-    out_ref,
+    from_plane,
+    from_line,
+    head_own,
     heads,
     parts,
     got,
     done,
     final,
+    pair_send,
+    pair_recv,
+    plane_send,
+    plane_recv,
+    line_send,
+    line_recv,
     head_send,
     head_recv,
     part_send,
@@ -362,18 +326,100 @@
     done_recv,
 ):
     kv_index, tp_index = lax.axis_index("kv"), lax.axis_index("tp")
-    depth = head_ref.shape[1]
-    width = parts.shape[2]
+    seqs, rank = fresh_ref.shape
+    lane = lax.broadcasted_iota(jnp.int32, (seqs, LANES), 1)
+    lines = kv_count // INNER
+    offsets = plane_offsets(tp_count)
+    sibling = (kv_index, sibling_of(tp_index))
+    planes = [plane_peer(kv_index, tp_index, tp_count, offset) for offset in offsets]
+    crossed = [plane for plane, offset in zip(planes, offsets) if offset[0] > 0 and offset[1] > 0]
     tp_peers = [(kv_index, lax.rem(tp_index + step, tp_count)) for step in range(1, tp_count)]
     kv_peers = [(lax.rem(kv_index + step, kv_count), tp_index) for step in range(1, kv_count)]
-    greet(tp_peers + kv_peers)
+    greet(tp_peers + kv_peers + crossed)
+
+    def shifted(kv_at, step):
+        return lax.rem(kv_at + INNER * step, kv_count)
+
+    order = [(slot, line) for slot in range(len(offsets) - 1, 0, -1) for line in range(1, lines)]
+    order += [(slot, 0) for slot in range(len(offsets) - 1, 0, -1)]
+    order += [(0, line) for line in list(range(lines - 1, 0, -1)) + [0]]
+    pair_copies, plane_copies, line_copies = {}, {}, {}
+    for slot, line in order:
+        kv_at, tp_at = shifted(planes[slot][0], line), planes[slot][1]
+        pair_copies[slot, line] = remote(
+            part_ref.at[kv_at * tp_count + sibling_of(tp_at)],
+            from_pair.at[slot, line],
+            pair_send.at[slot, line],
+            pair_recv.at[slot, line],
+            sibling,
+        )
+        pair_copies[slot, line].start()
+
+    def put(slot, line, term):
+        values, top, total = term
+        merged[slot, line, :, :rank] = values.astype(merged.dtype)
+        merged[slot, line, :, rank:] = stats_lanes(top, total, lane, narrow).astype(merged.dtype)
+
+    own = None
+    for slot, line in order:
+        kv_at, tp_at = shifted(planes[slot][0], line), planes[slot][1]
+        pair_copies[slot, line].wait_recv()
+        term = merge(
+            split_stats(part_ref[kv_at * tp_count + tp_at], rank),
+            split_stats(from_pair[slot, line], rank),
+        )
+        if slot > 0:
+            put(slot, line, term)
+            plane_copies[slot, line] = remote(
+                merged.at[slot, line],
+                from_plane.at[slot, line],
+                plane_send.at[slot, line],
+                plane_recv.at[slot, line],
+                planes[slot],
+            )
+            plane_copies[slot, line].start()
+            continue
+        for side in range(1, len(offsets)):
+            plane_copies[side, line].wait_recv()
+            term = merge(term, split_stats(from_plane[side, line], rank))
+        if line == 0:
+            own = term
+            continue
+        put(slot, line, term)
+        line_copies[line] = remote(
+            merged.at[slot, line],
+            from_line.at[line],
+            line_send.at[line],
+            line_recv.at[line],
+            (shifted(kv_index, line), tp_index),
+        )
+        line_copies[line].start()
+    for line in range(1, lines):
+        line_copies[line].wait_recv()
+        own = merge(own, split_stats(from_line[line], rank))
+    values, old_top, total = own
+    own_score = own_ref[:, 0:1]
+    top = jnp.maximum(old_top, own_score)
+    old_scale, own_weight = jnp.exp(old_top - top), jnp.exp(own_score - top)
+    latent_out = (values * old_scale + own_weight * fresh_ref[...].astype(jnp.float32)) / (
+        total * old_scale + own_weight
+    )
+    high = latent_out.astype(jnp.bfloat16)
+    low = (latent_out - high.astype(jnp.float32)).astype(jnp.bfloat16)
+    head_out = jnp.dot(high, value_ref[...], preferred_element_type=jnp.float32) + jnp.dot(
+        low, value_ref[...], preferred_element_type=jnp.float32
+    )
+    head_own[...] = head_out.astype(jnp.bfloat16)
+
+    depth = head_own.shape[1]
+    width = parts.shape[2]
     copies = []
     for step, peer in enumerate(tp_peers):
         copies.append(
-            remote(head_ref, heads.at[tp_index], head_send.at[step], head_recv.at[step], peer)
+            remote(head_own, heads.at[tp_index], head_send.at[step], head_recv.at[step], peer)
         )
         copies[-1].start()
-    heads[tp_index] = head_ref[...]
+    heads[tp_index] = head_own[...]
     for copy in copies:
         copy.wait()
     total = jnp.dot(heads[0], weight_ref[:depth, :], preferred_element_type=jnp.float32)
@@ -413,33 +459,41 @@
         copy.wait()
     for at in range(kv_count):
         out_ref[:, at * width : (at + 1) * width] = final[at]
-
-
-def project_out(head_out, weight, kv_count, tp_count):
-    seqs, depth = head_out.shape
+    for copy in list(pair_copies.values()) + list(plane_copies.values()) + list(
+        line_copies.values()
+    ):
+        copy.wait_send()
+
+
+def scatter_project(part, own, fresh, value, weight, kv_count, tp_count):
+    _, seqs, block = part.shape
     columns = weight.shape[1]
     width = columns // kv_count
+    depth = value.shape[1]
+    lines, planes = kv_count // INNER, INNER * tp_count // 2
+    semaphores = [(planes, lines)] * 4 + [(lines,)] * 2
+    semaphores += [(tp_count - 1,)] * 2 + [(kv_count - 1,)] * 4
     return pl.pallas_call(
-        functools.partial(out_kernel, kv_count, tp_count),
+        functools.partial(scatter_kernel, kv_count, tp_count),
         out_shape=jax.ShapeDtypeStruct((seqs, columns), jnp.bfloat16),
-        in_specs=[pl.BlockSpec(memory_space=pltpu.VMEM)] * 2,
+        in_specs=[pl.BlockSpec(memory_space=pltpu.VMEM)] * 5,
         out_specs=pl.BlockSpec(memory_space=pltpu.VMEM),
         scratch_shapes=[
-            pltpu.VMEM((tp_count, seqs, depth), head_out.dtype),
+            pltpu.VMEM((planes, lines, seqs, block), part.dtype),
+            pltpu.VMEM((planes, lines, seqs, block), part.dtype),
+            pltpu.VMEM((planes, lines, seqs, block), part.dtype),
+            pltpu.VMEM((lines, seqs, block), part.dtype),
+            pltpu.VMEM((seqs, depth), jnp.bfloat16),
+            pltpu.VMEM((tp_count, seqs, depth), jnp.bfloat16),
             pltpu.VMEM((kv_count, seqs, width), jnp.float32),
             pltpu.VMEM((kv_count, seqs, width), jnp.float32),
             pltpu.VMEM((seqs, width), jnp.bfloat16),
             pltpu.VMEM((kv_count, seqs, width), jnp.bfloat16),
-            pltpu.SemaphoreType.DMA((tp_count - 1,)),
-            pltpu.SemaphoreType.DMA((tp_count - 1,)),
-            pltpu.SemaphoreType.DMA((kv_count - 1,)),
-            pltpu.SemaphoreType.DMA((kv_count - 1,)),
-            pltpu.SemaphoreType.DMA((kv_count - 1,)),
-            pltpu.SemaphoreType.DMA((kv_count - 1,)),
-        ],
-        compiler_params=pltpu.CompilerParams(collective_id=3, has_side_effects=True),
-        name="project_out",
-    )(head_out, weight)
+        ]
+        + [pltpu.SemaphoreType.DMA(shape) for shape in semaphores],
+        compiler_params=pltpu.CompilerParams(collective_id=2, has_side_effects=True),
+        name="scatter_project",
+    )(part, own, fresh, value, weight)
 
 
 def kernel_shards(
@@ -517,11 +571,13 @@
     new_latent = (
         fresh_f * lax.rsqrt(jnp.mean(fresh_f * fresh_f, axis=1, keepdims=True) + EPS) * latent_gain
     ).astype(jnp.bfloat16)
-    new_latent_f = new_latent.astype(jnp.float32)
-    own_score = (
-        jnp.einsum("bhr,br->bh", all_latent, new_latent, preferred_element_type=jnp.float32)
-        + jnp.einsum("bhq,bq->bh", all_rope, new_rotary, preferred_element_type=jnp.float32)
+    own_query = lax.dynamic_slice_in_dim(got_latent, device, 1, 0)[0].astype(jnp.float32)
+    own_rope = lax.dynamic_slice_in_dim(all_rope, device, 1, 1)[:, 0].astype(jnp.float32)
+    own = (
+        jnp.sum(own_query * new_latent.astype(jnp.float32), axis=1, keepdims=True)
+        + jnp.sum(own_rope * new_rotary.astype(jnp.float32), axis=1, keepdims=True)
     ) * score_scale
+    own = jnp.broadcast_to(own, (seq_count, LANES))
     pos_dev = cache_latent.shape[1]
     position = device * pos_dev + jnp.arange(pos_dev, dtype=jnp.int32)
     valid = position[None, :] < lengths[:, None]
@@ -530,7 +586,7 @@
         + jnp.einsum("bhq,bpq->bhp", all_rope, cache_rotary, preferred_element_type=jnp.float32)
     ) * score_scale
     masked = jnp.where(valid[:, None, :], scores, -jnp.inf)
-    local_top = jnp.maximum(jnp.max(masked, axis=2), own_score)
+    local_top = jnp.maximum(jnp.max(masked, axis=2), LOWEST)
     weights = jnp.where(valid[:, None, :], jnp.exp(scores - local_top[:, :, None]), 0.0)
     total_part = jnp.sum(weights, axis=2)
     summed_part = jnp.einsum(
@@ -542,17 +598,8 @@
     lane = lax.broadcasted_iota(jnp.int32, (seq_count, head_count, LANES), 2)
     stats = stats_lanes(local_top[:, :, None], total_part[:, :, None], lane, rounded)
     part = jnp.concatenate([summed_part, stats.astype(jnp.bfloat16)], axis=2).transpose(1, 0, 2)
-    block_sum, block_stats = scatter_sum(part, latent_rank, kv_count, tp_count)
-    own = lax.dynamic_slice_in_dim(own_score, device, 1, 1)
-    block_top, block_total = block_stats[:, 0:1], block_stats[:, 1:2]
-    top_score = jnp.maximum(block_top, own)
-    old_scale, own_weight = jnp.exp(block_top - top_score), jnp.exp(own - top_score)
-    latent_out = (block_sum * old_scale + own_weight * new_latent_f) / (
-        block_total * old_scale + own_weight
-    )
-    value_weight = lax.dynamic_slice_in_dim(w_value_up, device, 1, 1)
-    head_out = value_product(latent_out[:, None, :], value_weight).astype(jnp.bfloat16)
-    mixed_out = project_out(head_out[:, 0, :], w_out, kv_count, tp_count)
+    value_weight = lax.dynamic_slice_in_dim(w_value_up, device, 1, 1)[:, 0, :]
+    mixed_out = scatter_project(part, own, new_latent, value_weight, w_out, kv_count, tp_count)
     piece_width = latent_rank // (kv_count * tp_count)
     latent_piece = lax.dynamic_slice_in_dim(new_latent, device * piece_width, piece_width, 1)
     return (mixed_out, latent_piece, new_rotary)
@@ -564,6 +611,8 @@
     return (
         heads == kv_count * tp_count
         and tp_count % 2 == 0
+        and kv_count % INNER == 0
+        and kv_count > INNER
         and w_key_up.shape[0] // tp_count % LANES == 0
         and w_latent.shape[1] // kv_count % LANES == 0
         and heads // kv_count * w_rotary.shape[1] % LANES == 0

time: 110 us -> 93.2 us (0.85)
  Pallas kernels: 71.1 us -> 56.9 us
  matrix products: 16.7 us -> 12.9 us
  local copies, waits for them, and re-layouts: 6.16 us -> 8.48 us
    pallas_call x2 -> x1, Pallas kernels: 45.3 us -> 32.2 us  [scatter_project(): pl.pallas_call(functools.partial(scatter_kernel, kv_count, tp_count), out...]
    dot_general x4 -> x0, matrix products: 4.77 us -> none  [the longest x1 1.9 us: kernel_shards(): jnp.einsum('bhr,br->bh', all_latent, new_latent, preferred_element_type=j...]
    reduce_sum x0 -> x2, other arithmetic: none -> 2.35 us  [the longest x1 1.57 us: kernel_shards(): jnp.sum(own_query * new_latent.astype(jnp.float32), axis=1, keepdims=True)]
    convert_element_type x2 -> x0, other arithmetic: 1.56 us -> none  [kernel_shards(): new_latent = (fresh_f * lax.rsqrt(jnp.mean(fresh_f * fresh_f, axis=1, kee...]
    dynamic_slice x1 -> x2, local copies, waits for them, and re-layouts: 2.14 us -> 3.49 us  [the longest x1 2.13 us: kernel_shards(): value_weight = lax.dynamic_slice_in_dim(w_value_up, device, 1, 1)[:, 0, :]]
    unnamed x9 -> x6, local copies, waits for them, and re-layouts: 2.52 us -> 3.25 us
where the time goes in v2:
time: 93.2 us; the launch traced here: 92 us
  Pallas kernels  56.9 us (61%)
  other arithmetic  13 us (14%)
  matrix products  12.9 us (14%)
  local copies, waits for them, and re-layouts  8.48 us (9%)
    pallas_call x1, Pallas kernels, scatter_project(): pl.pallas_call(functools.partial(scatter_kernel, kv_count, tp_count), out...  32.2 us
    pallas_call x1, Pallas kernels, gather_all(): pl.pallas_call(functools.partial(gather_kernel, kv_count, tp_count), out_...  17.9 us
    pallas_call x1, Pallas kernels, tp_sum(): pl.pallas_call(functools.partial(tp_sum_kernel, tp_count), out_shape=jax....  6.83 us
    dot_general x1, matrix products, kernel_shards(): jnp.einsum('bhr,bpr->bhp', all_latent, cache_latent, preferred_element_ty...  4.03 us
    unnamed x6, local copies, waits for them, and re-layouts  3.25 us
    dot_general x1, matrix products, kernel_shards(): jnp.einsum('bhp,bpr->bhr', weights.astype(jnp.bfloat16), cache_latent, pr...  2.86 us
    dynamic_slice x1, local copies, waits for them, and re-layouts, kernel_shards(): value_weight = lax.dynamic_slice_in_dim(w_value_up, device, 1, 1)[:, 0, :]  2.13 us

profile of v2, /device:TPU:0, one launch (start us, length us, event | category | flops | bytes accessed | tf_op | source)
XLA Modules:
  0.0 92.0 jit_solution(513352712192323864)
XLA Ops:
  0.6 0.0 copy-start
  0.6 1.1 %copy-done = bf16[1024,4,96]{0,2,1:T(8,128)(2,1)S(1)} copy-done((bf16[1024,4,96]{0,2,1:T(8,128)(2,1)S(1)}, bf16[1024,4,96]{0,2,1:T(8,128)(2,1)}, u32[]{:S(2)}) %copy-start) | copy-done | bytes 786456
  1.8 1.1 %fusion.15 = f32[16,4,96]{2,0,1:T(8,128)S(1)} fusion(bf16[1024,4,96]{0,2,1:T(8,128)(2,1)S(1)} %copy-done, bf16[16,1024]{1,0:T(8,128)(2,1)} %param.12, f32[1024]{0:T(1024)} %param.13), kind=kOutput, calls=%fused_computation.30 | convolution fusion | flops 12632064 | bytes 847872 | tf_op jit(solution)/shard_map/bd,dhn->bhn/dot_general | solution.py:528
  2.9 0.0 copy-start.1
  2.9 0.1 reshape.154
  3.0 0.9 fusion.10
  3.9 0.1 broadcast_in_dim.79
  4.0 1.0 %fusion.17 = f32[16,32]{1,0:T(8,128)S(1)} fusion(bf16[1024,32]{0,1:T(8,128)(2,1)} %param.16, bf16[16,1024]{1,0:T(8,128)(2,1)} %param.12, f32[1024]{0:T(1024)} %param.13), kind=kOutput, calls=%fused_computation.35 | convolution fusion | flops 1097728 | bytes 104448 | tf_op jit(solution)/shard_map/dot_general | solution.py:530
  5.0 1.1 %fusion.19 = f32[16,128]{1,0:T(8,128)S(1)} fusion(bf16[1024,128]{1,0:T(8,128)(2,1)} %param.15, bf16[16,1024]{1,0:T(8,128)(2,1)} %param.12, f32[1024]{0:T(1024)} %param.13), kind=kOutput, calls=%fused_computation.36 | convolution fusion | flops 4243456 | bytes 307200 | tf_op jit(solution)/shard_map/dot_general | solution.py:529
  6.1 0.7 pad_maximum_fusion.part_ref
  6.8 6.8 %tp_sum.1 = f32[16,640]{1,0:T(8,128)} custom-call(f32[16,640]{1,0:T(8,128)} %pad_maximum_fusion.part_ref), custom_call_target="tpu_custom_call" | custom-call | tf_op jit(solution)/shard_map/tp_sum/pallas_call | solution.py:81
  13.6 0.9 rsqrt_reduce_fusion
  14.5 0.8 slice_multiply_fusion
  15.3 0.7 convert_element_type.76
  16.0 0.1 subtract_convert_fusion.1
  16.1 0.8 multiply_convert_fusion
  16.9 0.1 reshape.155
  17.0 0.1 slice_convert_fusion
  17.1 0.1 subtract_convert_fusion
  17.2 0.1 pad_maximum_fusion.1
  17.3 0.1 convert_element_type.77
  17.4 0.8 multiply_convert_fusion.1
  18.1 0.6 pad_maximum_fusion.2.extra_ref
  18.7 1.7 %convolution_convert_fusion.query_ref = bf16[4,16,256]{2,1,0:T(8,128)(2,1)} fusion(bf16[256,4,64]{0,2,1:T(8,128)(2,1)} %param.18, bf16[16,4,64]{2,1,0:T(4,128)(2,1)S(1)} %bitcast.40), kind=kOutput, calls=%fused_computation.2 | convolution fusion | flops 2113536 | bytes 172032 | tf_op jit(solution)/shard_map/bhn,rhn->hbr/dot_general | solution.py:558
  20.4 17.9 %gather_all.1 = (bf16[32,16,1024]{2,1,0:T(8,128)(2,1)}, bf16[8,16,256]{2,1,0:T(8,128)(2,1)}) custom-call(bf16[4,16,256]{2,1,0:T(8,128)(2,1)} %convolution_convert_fusion.query_ref, bf16[16,256]{1,0:T(8,128)(2,1)} %pad_maximum_fusion.2.extra_ref), custom_call_target="tpu_custom_call" | custom-call | tf_op jit(solution)/shard_map/gather_all/pallas_call | solution.py:234
  38.3 0.8 convert_bitcast_fusion
  39.1 0.9 fusion.11
  40.0 1.6 %fusion.14 = (f32[16]{0:T(128)S(1)}, bf16[16,1024]{1,0:T(8,128)(2,1)}) fusion(bf16[32,16,1024]{2,1,0:T(8,128)(2,1)} %get-tuple-element.5, s32[]{:T(128)S(6)} %select_n.39, f32[1024]{0:T(1024)} %param.17, f32[16]{0:T(128)S(1)} %add_rsqrt_fusion, f32[8,2,8,128]{3,2,1,0:T(8,128)S(1)} %get-tuple-element.13), kind=kLoop, calls=%fused_computation.28 | loop fusion | flops 114672 | bytes 135300 | tf_op jit(solution)/shard_map/reduce_sum | solution.py:577
  41.6 0.1 reshape.156
  41.7 0.8 fusion.23
  42.5 0.7 broadcast_in_dim.87.own_ref
  43.2 1.1 %fusion.7 = f32[16,32,128]{2,1,0:T(8,128)S(1)} fusion(bf16[16,128,32]{1,2,0:T(8,128)(2,1)} %param.22, bf16[16,32,32]{2,0,1:T(8,128)(2,1)S(1)} %bitcast.38), kind=kOutput, calls=%fused_computation.15 | convolution fusion | flops 4194304 | bytes 425984 | tf_op jit(solution)/shard_map/bhq,bpq->bhp/dot_general | solution.py:586
  44.2 4.0 %fusion = f32[16,32,128]{2,1,0:T(8,128)S(1)} fusion(bf16[16,128,1024]{2,1,0:T(8,128)(2,1)} %param.21, bf16[16,32,1024]{2,0,1:T(8,128)(2,1)} %bitcast.35), kind=kOutput, calls=%fused_computation.3 | convolution fusion | flops 134217728 | bytes 5505024 | tf_op jit(solution)/shard_map/bhr,bpr->bhp/dot_general | solution.py:585
  48.3 0.0 copy-done.1
  48.3 0.1 broadcast_compare_fusion
  48.4 0.4 select_reduce_fusion
  48.8 0.4 fusion.4
  49.2 2.9 %fusion.5 = bf16[16,32,1024]{2,1,0:T(8,128)(2,1)S(1)} fusion(bf16[16,128,1024]{2,1,0:T(8,128)(2,1)} %param.21, bf16[16,32,128]{2,0,1:T(8,128)(2,1)S(1)} %get-tuple-element.11), kind=kOutput, calls=%fused_computation.13 | convolution fusion | flops 134217728 | bytes 5373952 | tf_op jit(solution)/shard_map/bhp,bpr->bhr/dot_general | solution.py:592
  52.1 0.6 copy.66
  52.7 0.4 select_convert_fusion
  53.1 1.1 %maximum_bitcast_fusion.part_ref = bf16[32,16,1152]{2,1,0:T(8,128)(2,1)} fusion(bf16[16,32,128]{2,0,1:T(8,128)(2,1)S(1)} %select_convert_fusion, bf16[16,32,1024]{2,0,1:T(8,128)(2,1)S(1)} %copy.66), kind=kLoop, calls=%fused_computation.1 | loop fusion | flops 2359296 | bytes 2359296 | tf_op jit(solution)/shard_map/transpose | solution.py:600
  54.2 2.1 %constant_dynamic-slice_fusion.1 = bf16[1024,1,128]{2,1,0:T(2,128)(2,1)S(1)} fusion(bf16[1024,32,128]{2,1,0:T(8,128)(2,1)} %param.19, s32[]{:T(128)S(6)} %select_n.39), kind=kLoop, calls=%fused_computation.57 | loop fusion | bytes 524292 | tf_op jit(solution)/shard_map/dynamic_slice | solution.py:601
  56.4 0.7 copy.68
  57.1 32.2 %scatter_project.1 = bf16[16,1024]{1,0:T(8,128)(2,1)} custom-call(bf16[32,16,1152]{2,1,0:T(8,128)(2,1)} %maximum_bitcast_fusion.part_ref, f32[16,128]{1,0:T(8,128)} %broadcast_in_dim.87.own_ref, bf16[16,1024]{1,0:T(8,128)(2,1)} %get-tuple-element.10.fresh_ref, bf16[1024,128]{1,0:T(8,128)(2,1)} %bitcast.36, bf16[512,1024]{1,0:T(8,128)(2,1)} %weight_ref.1), custom_call_target="tpu_custom_call" | custom-call | tf_op jit(solution)/shard_map/scatter_project/pallas_call | solution.py:476
  89.3 1.4 %constant_dynamic-slice_fusion = bf16[16,32]{1,0:T(8,128)(2,1)} fusion(bf16[16,1024]{1,0:T(8,128)(2,1)} %get-tuple-element.10.fresh_ref, s32[]{:T(128)S(6)} %select_n.40), kind=kLoop, calls=%fused_computation.56 | loop fusion | bytes 2052 | tf_op jit(solution)/shard_map/dynamic_slice | solution.py:604
  90.7 1.4 %copy.70 = bf16[16,1024]{1,0:T(8,128)(2,1)} copy(bf16[16,1024]{1,0:T(8,128)(2,1)} %scatter_project.1) | data formatting | bytes 65536
  (11 shorter events, 0.1 us)
Async XLA Ops:
  0.6 1.1 %copy-start = (bf16[1024,4,96]{0,2,1:T(8,128)(2,1)S(1)}, bf16[1024,4,96]{0,2,1:T(8,128)(2,1)}, u32[]{:S(2)}) copy-start(bf16[1024,4,96]{0,2,1:T(8,128)(2,1)} %param.14) | copy-start | bytes 2359300
  2.9 45.4 %copy-start.1 = (s32[16]{0:T(128)S(1)}, s32[16]{0:T(128)}, u32[]{:S(2)}) copy-start(s32[16]{0:T(128)} %param.23) | copy-start | bytes 196

commit v3 on v2

--- a/solution.py
+++ b/solution.py
@@ -61,7 +61,9 @@
     )
 
 
-def tp_sum_kernel(tp_count, part_ref, sum_ref, slots, send, recv):
+def tp_sum_kernel(
+    tp_count, model_width, square_at, part_ref, query_ref, latent_ref, rest_ref, slots, send, recv
+):
     kv_index, tp_index = lax.axis_index("kv"), lax.axis_index("tp")
     peers = [(kv_index, lax.rem(tp_index + step, tp_count)) for step in range(1, tp_count)]
     greet(peers)
@@ -74,15 +76,27 @@
     slots[tp_index] = part_ref[...]
     for copy in copies:
         copy.wait()
-    sum_ref[...] = jnp.sum(slots[...], axis=0)
-
-
-def tp_sum(part, tp_count):
+    total = jnp.sum(slots[...], axis=0)
+    total = total * lax.rsqrt(total[:, square_at : square_at + 1] / model_width + EPS)
+    query_width = query_ref.shape[1]
+    rest_at = query_width + latent_ref.shape[1]
+    query_ref[...] = total[:, :query_width].astype(query_ref.dtype)
+    latent_ref[...] = total[:, query_width:rest_at].astype(latent_ref.dtype)
+    rest_ref[...] = total[:, rest_at:]
+
+
+def tp_sum(part, tp_count, model_width, query_width, latent_width, rope_width):
+    seqs, width = part.shape
+    rest_at = query_width + latent_width
     return pl.pallas_call(
-        functools.partial(tp_sum_kernel, tp_count),
-        out_shape=jax.ShapeDtypeStruct(part.shape, part.dtype),
+        functools.partial(tp_sum_kernel, tp_count, model_width, rest_at + rope_width),
+        out_shape=(
+            jax.ShapeDtypeStruct((seqs, query_width), jnp.bfloat16),
+            jax.ShapeDtypeStruct((seqs, latent_width), jnp.bfloat16),
+            jax.ShapeDtypeStruct((seqs, width - rest_at), jnp.float32),
+        ),
         in_specs=[pl.BlockSpec(memory_space=pltpu.VMEM)],
-        out_specs=pl.BlockSpec(memory_space=pltpu.VMEM),
+        out_specs=(pl.BlockSpec(memory_space=pltpu.VMEM),) * 3,
         scratch_shapes=[
             pltpu.VMEM((tp_count,) + part.shape, part.dtype),
             pltpu.SemaphoreType.DMA((tp_count - 1,)),
@@ -541,17 +555,11 @@
         ],
         axis=1,
     )
-    packed = tp_sum(packed, tp_count)
-    query_sum, latent_sum, rotary_sum, square_sum = jnp.split(
-        packed,
-        [query_width, query_width + latent_width, query_width + latent_width + rope_width],
-        axis=1,
-    )
-    inverse = lax.rsqrt(square_sum[:, :1] / model_width + EPS)
-    query_heads = (query_sum * inverse).astype(jnp.bfloat16)
+    query_heads, compressed, rest = tp_sum(
+        packed, tp_count, model_width, query_width, latent_width, rope_width
+    )
     query_heads = query_heads.reshape(seq_count, heads_dev, w_query.shape[2])
-    compressed = (latent_sum * inverse).astype(jnp.bfloat16)
-    new_rotary = rotate(rotary_sum * inverse, lengths).astype(jnp.bfloat16)
+    new_rotary = rotate(rest[:, :rope_width], lengths).astype(jnp.bfloat16)
     query_rope = rotate(query_heads[:, :, nope_width:].astype(jnp.float32), lengths).astype(
         jnp.bfloat16
     )
@@ -577,7 +585,6 @@
         jnp.sum(own_query * new_latent.astype(jnp.float32), axis=1, keepdims=True)
         + jnp.sum(own_rope * new_rotary.astype(jnp.float32), axis=1, keepdims=True)
     ) * score_scale
-    own = jnp.broadcast_to(own, (seq_count, LANES))
     pos_dev = cache_latent.shape[1]
     position = device * pos_dev + jnp.arange(pos_dev, dtype=jnp.int32)
     valid = position[None, :] < lengths[:, None]
@@ -613,6 +620,7 @@
         and tp_count % 2 == 0
         and kv_count % INNER == 0
         and kv_count > INNER
+        and heads // kv_count * w_query.shape[2] % LANES == 0
         and w_key_up.shape[0] // tp_count % LANES == 0
         and w_latent.shape[1] // kv_count % LANES == 0
         and heads // kv_count * w_rotary.shape[1] % LANES == 0

time: 93.2 us -> 92.1 us (0.988)
  other arithmetic: 13 us -> 11.2 us
    convert_element_type x2 -> x0, other arithmetic: 1.58 us -> none  [the longest x1 0.81 us: kernel_shards(): query_heads = (query_sum * inverse).astype(jnp.bfloat16)]
where the time goes in v3:
time: 92.1 us; the launch traced here: 91 us
  Pallas kernels  57 us (62%)
  matrix products  12.9 us (14%)
  other arithmetic  11.2 us (12%)
  local copies, waits for them, and re-layouts  9.19 us (10%)
    pallas_call x1, Pallas kernels, scatter_project(): pl.pallas_call(functools.partial(scatter_kernel, kv_count, tp_count), out...  32.2 us
    pallas_call x1, Pallas kernels, gather_all(): pl.pallas_call(functools.partial(gather_kernel, kv_count, tp_count), out_...  17.9 us
    pallas_call x1, Pallas kernels, tp_sum(): pl.pallas_call(functools.partial(tp_sum_kernel, tp_count, model_width, re...  6.91 us
    dot_general x1, matrix products, kernel_shards(): jnp.einsum('bhr,bpr->bhp', all_latent, cache_latent, preferred_element_ty...  4.03 us
    unnamed x6, local copies, waits for them, and re-layouts  3.25 us
    dot_general x1, matrix products, kernel_shards(): jnp.einsum('bhp,bpr->bhr', weights.astype(jnp.bfloat16), cache_latent, pr...  2.86 us
    dynamic_slice x1, local copies, waits for them, and re-layouts, kernel_shards(): value_weight = lax.dynamic_slice_in_dim(w_value_up, device, 1, 1)[:, 0, :]  2.13 us

profile of v3, /device:TPU:0, one launch (start us, length us, event | category | flops | bytes accessed | tf_op | source)
XLA Modules:
  0.0 91.0 jit_solution(15222480844159157409)
XLA Ops:
  0.6 0.0 copy-start
  0.6 1.1 %copy-done = bf16[1024,4,96]{0,2,1:T(8,128)(2,1)S(1)} copy-done((bf16[1024,4,96]{0,2,1:T(8,128)(2,1)S(1)}, bf16[1024,4,96]{0,2,1:T(8,128)(2,1)}, u32[]{:S(2)}) %copy-start) | copy-done | bytes 786456
  1.8 1.1 %fusion.15 = f32[16,4,96]{2,0,1:T(8,128)S(1)} fusion(bf16[1024,4,96]{0,2,1:T(8,128)(2,1)S(1)} %copy-done, bf16[16,1024]{1,0:T(8,128)(2,1)} %param.12, f32[1024]{0:T(1024)} %param.13), kind=kOutput, calls=%fused_computation.30 | convolution fusion | flops 12632064 | bytes 847872 | tf_op jit(solution)/shard_map/bd,dhn->bhn/dot_general | solution.py:542
  2.9 0.0 copy-start.1
  2.9 0.1 reshape.165
  3.0 0.9 fusion.10
  3.9 0.1 broadcast_in_dim.74
  4.0 1.0 %fusion.17 = f32[16,32]{1,0:T(8,128)S(1)} fusion(bf16[1024,32]{0,1:T(8,128)(2,1)} %param.16, bf16[16,1024]{1,0:T(8,128)(2,1)} %param.12, f32[1024]{0:T(1024)} %param.13), kind=kOutput, calls=%fused_computation.34 | convolution fusion | flops 1097728 | bytes 104448 | tf_op jit(solution)/shard_map/dot_general | solution.py:544
  5.0 1.1 %fusion.19 = f32[16,128]{1,0:T(8,128)S(1)} fusion(bf16[1024,128]{1,0:T(8,128)(2,1)} %param.15, bf16[16,1024]{1,0:T(8,128)(2,1)} %param.12, f32[1024]{0:T(1024)} %param.13), kind=kOutput, calls=%fused_computation.35 | convolution fusion | flops 4243456 | bytes 307200 | tf_op jit(solution)/shard_map/dot_general | solution.py:543
  6.1 0.7 pad_maximum_fusion.part_ref
  6.8 6.9 %tp_sum.1 = (bf16[16,384]{1,0:T(8,128)(2,1)}, bf16[16,128]{1,0:T(8,128)(2,1)}, f32[16,128]{1,0:T(8,128)}) custom-call(f32[16,640]{1,0:T(8,128)} %pad_maximum_fusion.part_ref), custom_call_target="tpu_custom_call" | custom-call | tf_op jit(solution)/shard_map/tp_sum/pallas_call | solution.py:91
  13.7 0.7 convert_element_type.69
  14.4 0.9 subtract_convert_fusion.1
  15.3 0.8 reshape.166
  16.1 0.1 slice_convert_fusion
  16.2 0.1 subtract_convert_fusion
  16.3 0.1 pad_maximum_fusion.1
  16.3 0.1 convert_element_type.70
  16.4 1.3 %pad_maximum_fusion.2.extra_ref = bf16[16,256]{1,0:T(8,128)(2,1)} fusion(bf16[16,128]{1,0:T(8,128)(2,1)} %get-tuple-element.9, bf16[16,128]{1,0:T(8,128)(2,1)S(1)} %convert_element_type.70), kind=kLoop, calls=%fused_computation.41 | loop fusion | flops 16384 | bytes 16384 | tf_op jit(solution)/shard_map/concatenate | solution.py:571
  17.7 1.7 %convolution_convert_fusion.query_ref = bf16[4,16,256]{2,1,0:T(8,128)(2,1)} fusion(bf16[256,4,64]{0,2,1:T(8,128)(2,1)} %param.18, bf16[16,4,64]{2,1,0:T(4,128)(2,1)S(1)} %bitcast.42), kind=kOutput, calls=%fused_computation.2 | convolution fusion | flops 2113536 | bytes 172032 | tf_op jit(solution)/shard_map/bhn,rhn->hbr/dot_general | solution.py:566
  19.4 17.9 %gather_all.1 = (bf16[32,16,1024]{2,1,0:T(8,128)(2,1)}, bf16[8,16,256]{2,1,0:T(8,128)(2,1)}) custom-call(bf16[4,16,256]{2,1,0:T(8,128)(2,1)} %convolution_convert_fusion.query_ref, bf16[16,256]{1,0:T(8,128)(2,1)} %pad_maximum_fusion.2.extra_ref), custom_call_target="tpu_custom_call" | custom-call | tf_op jit(solution)/shard_map/gather_all/pallas_call | solution.py:248
  37.3 0.8 convert_bitcast_fusion
  38.1 0.9 fusion.11
  39.0 1.6 %fusion.14 = (f32[16]{0:T(128)S(1)}, bf16[16,1024]{1,0:T(8,128)(2,1)}) fusion(bf16[32,16,1024]{2,1,0:T(8,128)(2,1)} %get-tuple-element.10, s32[]{:T(128)S(6)} %select_n.39, f32[1024]{0:T(1024)} %param.17, f32[16]{0:T(128)S(1)} %add_rsqrt_fusion, f32[8,2,8,128]{3,2,1,0:T(8,128)S(1)} %get-tuple-element.19), kind=kLoop, calls=%fused_computation.28 | loop fusion | flops 114672 | bytes 135300 | tf_op jit(solution)/shard_map/reduce_sum | solution.py:585
  40.5 0.1 reshape.167
  40.7 0.8 fusion.23
  41.5 0.7 copy.37.own_ref
  42.2 1.1 %fusion.7 = f32[16,32,128]{2,1,0:T(8,128)S(1)} fusion(bf16[16,128,32]{1,2,0:T(8,128)(2,1)} %param.22, bf16[16,32,32]{2,0,1:T(8,128)(2,1)S(1)} %bitcast.40), kind=kOutput, calls=%fused_computation.15 | convolution fusion | flops 4194304 | bytes 425984 | tf_op jit(solution)/shard_map/bhq,bpq->bhp/dot_general | solution.py:593
  43.2 4.0 %fusion = f32[16,32,128]{2,1,0:T(8,128)S(1)} fusion(bf16[16,128,1024]{2,1,0:T(8,128)(2,1)} %param.21, bf16[16,32,1024]{2,0,1:T(8,128)(2,1)} %bitcast.37), kind=kOutput, calls=%fused_computation.3 | convolution fusion | flops 134217728 | bytes 5505024 | tf_op jit(solution)/shard_map/bhr,bpr->bhp/dot_general | solution.py:592
  47.3 0.0 copy-done.1
  47.3 0.1 broadcast_compare_fusion
  47.4 0.4 select_reduce_fusion
  47.8 0.4 fusion.4
  48.2 2.9 %fusion.5 = bf16[16,32,1024]{2,1,0:T(8,128)(2,1)S(1)} fusion(bf16[16,128,1024]{2,1,0:T(8,128)(2,1)} %param.21, bf16[16,32,128]{2,0,1:T(8,128)(2,1)S(1)} %get-tuple-element.17), kind=kOutput, calls=%fused_computation.13 | convolution fusion | flops 134217728 | bytes 5373952 | tf_op jit(solution)/shard_map/bhp,bpr->bhr/dot_general | solution.py:599
  51.1 0.6 copy.68
  51.7 0.4 select_convert_fusion
  52.1 1.1 %maximum_bitcast_fusion.part_ref = bf16[32,16,1152]{2,1,0:T(8,128)(2,1)} fusion(bf16[16,32,128]{2,0,1:T(8,128)(2,1)S(1)} %select_convert_fusion, bf16[16,32,1024]{2,0,1:T(8,128)(2,1)S(1)} %copy.68), kind=kLoop, calls=%fused_computation.1 | loop fusion | flops 2359296 | bytes 2359296 | tf_op jit(solution)/shard_map/transpose | solution.py:607
  53.2 2.1 %constant_dynamic-slice_fusion.1 = bf16[1024,1,128]{2,1,0:T(2,128)(2,1)S(1)} fusion(bf16[1024,32,128]{2,1,0:T(8,128)(2,1)} %param.19, s32[]{:T(128)S(6)} %select_n.39), kind=kLoop, calls=%fused_computation.53 | loop fusion | bytes 524292 | tf_op jit(solution)/shard_map/dynamic_slice | solution.py:608
  55.4 0.7 copy.70
  56.1 32.2 %scatter_project.1 = bf16[16,1024]{1,0:T(8,128)(2,1)} custom-call(bf16[32,16,1152]{2,1,0:T(8,128)(2,1)} %maximum_bitcast_fusion.part_ref, f32[16,1]{1,0:T(8,128)} %copy.37.own_ref, bf16[16,1024]{1,0:T(8,128)(2,1)} %get-tuple-element.16.fresh_ref, bf16[1024,128]{1,0:T(8,128)(2,1)} %bitcast.38, bf16[512,1024]{1,0:T(8,128)(2,1)} %weight_ref.1), custom_call_target="tpu_custom_call" | custom-call | tf_op jit(solution)/shard_map/scatter_project/pallas_call | solution.py:490
  88.3 1.4 %constant_dynamic-slice_fusion = bf16[16,32]{1,0:T(8,128)(2,1)} fusion(bf16[16,1024]{1,0:T(8,128)(2,1)} %get-tuple-element.16.fresh_ref, s32[]{:T(128)S(6)} %select_n.40), kind=kLoop, calls=%fused_computation.52 | loop fusion | bytes 2052 | tf_op jit(solution)/shard_map/dynamic_slice | solution.py:611
  89.7 1.4 %copy.72 = bf16[16,1024]{1,0:T(8,128)(2,1)} copy(bf16[16,1024]{1,0:T(8,128)(2,1)} %scatter_project.1) | data formatting | bytes 65536
  (11 shorter events, 0.1 us)
Async XLA Ops:
  0.6 1.1 %copy-start = (bf16[1024,4,96]{0,2,1:T(8,128)(2,1)S(1)}, bf16[1024,4,96]{0,2,1:T(8,128)(2,1)}, u32[]{:S(2)}) copy-start(bf16[1024,4,96]{0,2,1:T(8,128)(2,1)} %param.14) | copy-start | bytes 2359300
  2.9 44.4 %copy-start.1 = (s32[16]{0:T(128)S(1)}, s32[16]{0:T(128)}, u32[]{:S(2)}) copy-start(s32[16]{0:T(128)} %param.23) | copy-start | bytes 196
